TPU v7x, 128 devices: a whole 4x4x4 slice. The times are simulated.
128 devices in a mesh: kv: 16 (over z, y), tp: 8 (over x, core).
Axes of the slice: x: 4, y: 4, z: 4, core: 2. Of those that a mesh axis runs over, the one named last changes fastest.
Arguments:
- tokens: bfloat16 [4096, 4096], P('kv'), may hold values from -6 to 6
- norm_gain: float32 [4096], replicated, may hold values from 0.1 to 1.9
- w_query: bfloat16 [4096, 2048], P('kv', 'tp'), may hold values from -0.09375 to 0.09375
- w_forget: bfloat16 [4096, 2048], P('kv', 'tp'), may hold values from -0.09375 to 0.09375
- w_value: bfloat16 [4096, 2048], P('kv', 'tp'), may hold values from -0.09375 to 0.09375
- w_gate: bfloat16 [4096, 2048], P('kv', 'tp'), may hold values from -0.09375 to 0.09375
- lower_bound: float32 [2048], P('tp'), may hold values from 0 to 0.9
- head_gain: float32 [2048], P('tp'), may hold values from 0.1 to 1.9
- w_out: bfloat16 [2048, 4096], P('kv', 'tp'), may hold values from -0.125 to 0.125
- state: float32 [1024, 16, 128, 128], P('kv', 'tp'), may hold values from -4 to 4
- prev_forget: bfloat16 [1024, 4, 2048], P('kv', None, 'tp'), may hold values from -8 to 8
- prev_value: bfloat16 [1024, 4, 2048], P('kv', None, 'tp'), may hold values from -6 to 6
- accepted: int32 [1024], P('kv'), may hold values from 0 to 4
Outputs:
- mixed: bfloat16 [4096, 4096], P('kv', 'tp')
- taken_state: float32 [1024, 16, 128, 128], P('kv', 'tp')
All inputs are finite; a program needn't handle non-finite values.
Results may differ from a plain program's by a relative error of at most 0.015.
Values may be sent and summed in bfloat16 or wider, within the bound.
A program may use at most 128 MiB of HBM per device.

v0:
```python
import jax
import jax.numpy as jnp
from jax import lax
from jax.sharding import Mesh
from jax.sharding import PartitionSpec as P

KV = ("kv_0", "kv_1")


EPSILON = 1e-06


def in_one_piece(arrays, axis, dim, along):
    both = jnp.concatenate(arrays, axis=along)
    filled, at, finished = (lax.all_gather(both, axis, axis=dim, tiled=True), 0, [])
    for a in arrays:
        finished.append(lax.slice_in_dim(filled, at, at + a.shape[along], axis=along))
        at += a.shape[along]
    return tuple(finished)


def sent_to_all(array, axis):
    size = lax.axis_size(axis)
    return lax.all_to_all(
        jnp.broadcast_to(array[None], (size, *array.shape)), axis, 0, 0, tiled=True
    )


def joined_along(parts, dim):
    parts = jnp.moveaxis(parts, 0, dim)
    shape = parts.shape
    return parts.reshape(*shape[:dim], shape[dim] * shape[dim + 1], *shape[dim + 2 :])


def gathered_copies(array, axis, dim):
    parts = sent_to_all(array, axis)
    return joined_along(parts, dim)


def gathered_by_axis(array, axes, dim):
    if not axes:
        return array
    nearer = lax.all_gather(array, axes[-1], axis=dim, tiled=True)
    return gathered_by_axis(nearer, axes[:-1], dim)


def forget_of(pre_act, bounds):
    return bounds + (1.0 - bounds) * jax.nn.sigmoid(pre_act.astype(jnp.float32))


def recur_one(start_state, old_forget, old_values, accepted_count, queries, forget, new_values):
    carried = start_state
    for position in range(old_forget.shape[0]):
        kept_mask = position < accepted_count
        decay_rate = jnp.where(kept_mask, old_forget[position], 1.0)
        weight = jnp.where(kept_mask, 1.0 - old_forget[position], 0.0)
        carried = (
            decay_rate[:, :, None] * carried + weight[:, :, None] * old_values[position][:, None, :]
        )
    taken = carried
    outputs = []
    for position in range(queries.shape[0]):
        carried = (
            forget[position][:, :, None] * carried
            + (1.0 - forget[position])[:, :, None] * new_values[position][:, None, :]
        )
        outputs.append(jnp.einsum("hd,hde->he", queries[position], carried))
    return (taken, jnp.stack(outputs))


def finish(outputs, head_gain, gate_proj):
    scaled = outputs * lax.rsqrt(jnp.mean(outputs * outputs, axis=-1, keepdims=True) + EPSILON)
    flat = scaled.reshape(gate_proj.shape)
    return (flat * head_gain * jax.nn.silu(gate_proj.astype(jnp.float32))).astype(jnp.bfloat16)


def on_device(
    tokens,
    norm_gain,
    w_query,
    w_forget,
    w_value,
    w_gate,
    lower_bound,
    head_gain,
    w_out,
    state,
    prev_forget,
    prev_value,
    accepted,
):
    seq_here, heads_here, key_size, value_size = state.shape
    proposals = prev_forget.shape[1]
    floated = tokens.astype(jnp.float32)
    normed = (
        floated
        * lax.rsqrt(jnp.mean(floated * floated, axis=-1, keepdims=True) + EPSILON)
        * norm_gain
    ).astype(jnp.bfloat16)
    pieces = in_one_piece((w_query, w_forget, w_value, w_gate), KV, 0, 1)
    columns = normed
    products = tuple(
        (
            jnp.dot(columns, weight_piece, preferred_element_type=jnp.float32)
            for weight_piece in pieces
        )
    )
    query_proj, forget_proj, value_proj, gate_proj = (
        product.astype(jnp.bfloat16) for product in products
    )
    bounds = lower_bound.reshape(heads_here, key_size)
    queries = query_proj.astype(jnp.float32).reshape(
        seq_here, proposals, heads_here, key_size
    ) * key_size ** (-0.5)
    forget = forget_of(forget_proj.reshape(seq_here, proposals, heads_here, key_size), bounds)
    new_values = value_proj.astype(jnp.float32).reshape(seq_here, proposals, heads_here, value_size)
    old_forget = forget_of(prev_forget.reshape(seq_here, proposals, heads_here, key_size), bounds)
    old_values = prev_value.astype(jnp.float32).reshape(seq_here, proposals, heads_here, value_size)
    taken, outputs = jax.vmap(recur_one)(
        state, old_forget, old_values, accepted, queries, forget, new_values
    )
    head_out = finish(outputs, head_gain, gate_proj)
    gathered_heads = gathered_copies(head_out, "tp", 1)
    columns = gathered_heads
    mixed = jnp.dot(columns, gathered_by_axis(w_out, KV, 0), preferred_element_type=jnp.float32)
    return (mixed.astype(jnp.bfloat16), taken)


def solution(mesh):
    finer = Mesh(mesh.devices.reshape(4, 4, mesh.shape["tp"]), ("kv_0", "kv_1", "tp"))
    placed = (
        P(KV, None),
        P(),
        P(KV, "tp"),
        P(KV, "tp"),
        P(KV, "tp"),
        P(KV, "tp"),
        P("tp"),
        P("tp"),
        P(KV, "tp"),
        P(KV, "tp", None, None),
        P(KV, None, "tp"),
        P(KV, None, "tp"),
        P(KV),
    )
    return jax.shard_map(
        on_device,
        mesh=finer,
        in_specs=placed,
        out_specs=(P(KV, "tp"), P(KV, "tp", None, None)),
        check_vma=False,
    )
```

profile of v0, /device:TPU:1, one launch (start us, length us, event | category | flops | bytes accessed | tf_op | source)
XLA Modules:
  0.0 214.9 jit_solution(8344740964777853124)
XLA Ops:
  7.2 0.0 copy-start.6
  7.2 0.0 all-gather.3.cloned.1.call-start
  7.2 2.0 pad_maximum_fusion
  9.2 0.0 all-gather.3.cloned.1.call-update
  9.2 0.0 all-gather.5.cloned.1.call-start
  9.3 13.3 %all_gather.10 = bf16[512,512]{1,0:T(8,128)(2,1)} all-gather(bf16[128,512]{1,0:T(8,128)(2,1)} %param.21), channel_id=1, replica_groups=mesh['kv_0'=4,'kv_1'=4,'tp'=8] {'kv_1'}, dimensions={0}, use_global_device_ids=true | all-gather | bytes 655360 | tf_op jit(solution)/shard_map/all_gather | solution.py:43
  22.5 0.0 all-gather.5.cloned.1.call-update
  22.6 0.0 copy-start.1
  22.6 0.0 copy-start.7
  22.6 2.4 %fusion.6 = f32[256]{0:T(256)S(1)} fusion(bf16[256,4096]{1,0:T(8,128)(2,1)} %param.13), kind=kLoop, calls=%fused_computation.12 | loop fusion | flops 3145472 | bytes 2098176 | tf_op jit(solution)/shard_map/reduce_sum | solution.py:97
  25.0 1.1 add_divide_fusion
  26.1 0.2 reshape.161
  26.3 0.7 broadcast_subtract_fusion.4
  26.9 0.7 broadcast_compare_fusion
  27.6 1.0 reshape.150
  28.6 0.1 slice_bitcast_fusion.10
  28.7 56.0 %all-gather.3.cloned.1.call-done = bf16[4096,1024]{1,0:T(8,128)(2,1)} async-done(((bf16[256,1024]{1,0:T(8,128)(2,1)}), bf16[4096,1024]{1,0:T(8,128)(2,1)}) %all-gather.3.cloned.1.call-update) | async-done | bytes 8388624 | tf_op jit(solution)/shard_map/all_gather | solution.py:15
  84.7 3.0 %fusion.54 = f32[256,256]{1,0:T(8,128)S(1)} fusion(bf16[4096,1024]{1,0:T(8,128)(2,1)} %all-gather.3.cloned.1.call-done, bf16[256,4096]{1,0:T(8,128)(2,1)} %param.13, f32[4096]{0:T(1024)} %param.14, f32[256]{0:T(256)S(1)} %add_rsqrt_fusion.1), kind=kOutput, calls=%fused_computation.45 | convolution fusion | flops 541392896 | bytes 4473856 | tf_op jit(solution)/shard_map/dot_general | solution.py:104
  87.7 0.1 reshape.146
  87.9 0.1 fusion.71
  88.0 0.7 slice_bitcast_fusion.15
  88.7 0.1 fusion.75
  88.8 0.1 copy.87
  88.8 0.1 copy.88
  88.9 0.1 copy.89
  89.0 0.1 copy.90
  89.0 0.1 copy.91
  89.1 0.1 copy.93
  89.1 0.1 copy.95
  89.2 0.1 copy.97
  89.3 0.1 copy.99
  89.3 0.1 copy.84
  89.4 3.1 %fusion.60 = f32[256,256]{1,0:T(8,128)} fusion(bf16[4096,1024]{1,0:T(8,128)(2,1)} %all-gather.3.cloned.1.call-done, bf16[256,4096]{1,0:T(8,128)(2,1)S(1)} %copy-done.1, f32[4096]{0:T(1024)S(1)} %copy-done.7, f32[256]{0:T(256)S(1)} %add_rsqrt_fusion.1), kind=kOutput, calls=%fused_computation.47 | convolution fusion | flops 541196288 | bytes 4473856 | tf_op jit(solution)/shard_map/dot_general | solution.py:104
  92.5 1.1 reshape.152
  93.5 0.7 slice_bitcast_fusion.6
  94.3 3.2 %fusion.36 = f32[256,256]{1,0:T(8,128)} fusion(bf16[4096,1024]{1,0:T(8,128)(2,1)} %all-gather.3.cloned.1.call-done, bf16[256,4096]{1,0:T(8,128)(2,1)S(1)} %copy-done.1, f32[4096]{0:T(1024)} %param.14, f32[256]{0:T(256)S(1)} %add_rsqrt_fusion.1), kind=kOutput, calls=%fused_computation.39 | convolution fusion | flops 541261824 | bytes 4473856 | tf_op jit(solution)/shard_map/dot_general | solution.py:104
  97.5 1.1 mul.267
  98.6 0.1 fusion.83
  98.7 0.1 copy.101
  98.7 0.9 copy.100
  99.6 0.1 copy.103
  99.7 0.9 copy.102
  100.6 19.9 %multiply_add_fusion.3 = f32[64,2,128,128]{3,2,1,0:T(8,128)S(1)} fusion(f32[64,2,128,128]{3,2,1,0:T(8,128)} %param.22, f32[64,2,128]{2,1,0:T(2,128)S(1)} %get-tuple-element.35, f32[64,2,128]{2,1,0:T(2,128)S(1)} %copy.97, f32[64,2,128]{2,1,0:T(2,128)S(1)} %get-tuple-element.33, f32[64,2,128]{2,1,0:T(2,128)S(1)} %copy.95, ...), kind=kLoop, calls=%fused_computation.7 | loop fusion | flops 25165824 | bytes 17563648 | tf_op jit(solution)/shard_map/vmap()/add | solution.py:58
  120.4 0.0 copy-start
  120.5 0.0 copy-start.4
  120.5 0.0 copy-done.5
  120.5 11.7 %fusion.29 = f32[64,2,1,128]{3,2,1,0:T(1,128)S(1)} fusion(f32[64,2,128,1]{2,3,1,0:T(1,128)S(1)} %bitcast.132, f32[64,2,128,128]{3,2,1,0:T(8,128)S(1)} %multiply_add_fusion.3, f32[64,2,128]{2,1,0:T(2,128)S(1)} %copy-done.5, f32[64,2,128]{2,1,0:T(2,128)S(1)} %copy.101, f32[64,2,128]{2,1,0:T(2,128)S(1)} %copy.100, f32[64,2,128]{2,1,0:T(2,128)S(1)} %get-tuple-element.22, ...), kind=kOutput, calls=%fused_computation.35 | convolution fusion | flops 16777216 | bytes 8912896 | tf_op jit(solution)/shard_map/vmap(hd,hde->he)/dot_general | solution.py:67
  132.1 19.0 %fusion.5 = f32[64,2,1,128]{3,2,1,0:T(1,128)S(1)} fusion(f32[64,2,128,1]{2,3,1,0:T(1,128)S(1)} %bitcast.131, f32[64,2,128]{2,1,0:T(2,128)S(1)} %copy-done.4, f32[64,2,128]{2,1,0:T(2,128)S(1)} %copy.103, f32[64,2,128]{2,1,0:T(2,128)S(1)} %copy.102, f32[64,2,128,128]{3,2,1,0:T(8,128)S(1)} %multiply_add_fusion.3, f32[64,2,128]{2,1,0:T(2,128)S(1)} %copy-done.5, ...), kind=kOutput, calls=%fused_computation.9 | convolution fusion | flops 23068672 | bytes 9109504 | tf_op jit(solution)/shard_map/vmap(hd,hde->he)/dot_general | solution.py:67
  151.1 5.8 %fusion.4 = f32[64,2,1,128]{3,2,1,0:T(1,128)S(1)} fusion(f32[64,2,128,1]{2,3,1,0:T(1,128)S(1)} %bitcast.122, f32[64,2,128,128]{3,2,1,0:T(8,128)S(1)} %multiply_add_fusion.3, f32[64,2,128]{2,1,0:T(2,128)S(1)} %get-tuple-element.22, f32[64,2,128]{2,1,0:T(2,128)S(1)} %copy.99, f32[64,2,128]{2,1,0:T(2,128)S(1)} %copy.84), kind=kOutput, calls=%fused_computation.8 | convolution fusion | flops 10485760 | bytes 8716288 | tf_op jit(solution)/shard_map/vmap(hd,hde->he)/dot_general | solution.py:67
  156.9 0.1 copy.105
  157.0 0.1 copy.104
  157.0 0.0 copy-start.8
  157.1 0.0 copy-start.9
  157.1 23.3 %fusion = f32[64,2,1,128]{3,2,1,0:T(1,128)S(1)} fusion(f32[64,2,128,1]{2,3,1,0:T(1,128)S(1)} %bitcast.130, f32[64,2,128]{2,1,0:T(2,128)S(1)} %copy-done.3, f32[64,2,128]{2,1,0:T(2,128)S(1)} %copy.105, f32[64,2,128]{2,1,0:T(2,128)S(1)} %copy.104, f32[64,2,128]{2,1,0:T(2,128)S(1)} %copy-done.4, f32[64,2,128]{2,1,0:T(2,128)S(1)} %copy.103, ...), kind=kOutput, calls=%fused_computation | convolution fusion | flops 29360128 | bytes 9306112 | tf_op jit(solution)/shard_map/vmap(hd,hde->he)/dot_general | solution.py:67
  180.3 0.5 multiply_reduce_fusion
  180.8 0.1 copy.106
  180.9 0.2 copy.107
  181.1 0.3 broadcast_multiply_fusion
  181.4 2.4 %fusion.70 = bf16[256,256]{1,0:T(8,128)(2,1)S(1)} fusion(f32[32,8,2,128]{3,2,1,0:T(2,128)S(1)} %bitcast.123, bf16[4096,1024]{1,0:T(8,128)(2,1)} %all-gather.3.cloned.1.call-done, f32[256]{0:T(256)S(1)} %copy-done.9, bf16[256,4096]{1,0:T(8,128)(2,1)S(1)} %copy-done.1, f32[4096]{0:T(1024)S(1)} %copy-done.8, f32[256]{0:T(256)S(1)} %add_rsqrt_fusion.1), kind=kOutput, calls=%fused_computation.53 | convolution fusion | flops 541655040 | bytes 4605952 | tf_op jit(solution)/shard_map/dot_general | solution.py:104
  183.8 0.1 copy.108
  183.9 1.0 broadcast_in_dim.60
  185.0 5.1 %all-to-all-start = ((bf16[8,256,256]{1,2,0:T(8,128)(2,1)}), bf16[8,256,256]{1,2,0:T(8,128)(2,1)S(1)}, u32[]{:S(2)}, u32[]{:S(2)}) async-start(bf16[8,256,256]{1,2,0:T(8,128)(2,1)} %broadcast_in_dim.60), calls=%async_computation | async-start | bytes 2097152 | tf_op jit(solution)/shard_map/all_to_all | solution.py:24
  190.1 15.0 %all-to-all-done = bf16[8,256,256]{1,2,0:T(8,128)(2,1)S(1)} async-done(((bf16[8,256,256]{1,2,0:T(8,128)(2,1)}), bf16[8,256,256]{1,2,0:T(8,128)(2,1)S(1)}, u32[]{:S(2)}, u32[]{:S(2)}) %all-to-all-start) | async-done | bytes 1048608 | tf_op jit(solution)/shard_map/all_to_all | solution.py:24
  205.0 3.0 %convolution_convert_fusion = bf16[256,512]{1,0:T(8,128)(2,1)} fusion(bf16[256,2048]{0,1:T(8,128)(2,1)S(1)} %bitcast.119, bf16[2048,512]{1,0:T(8,128)(2,1)} %all-gather.5.cloned.1.call-done), kind=kOutput, calls=%fused_computation.36 | convolution fusion | flops 537001984 | bytes 3407872 | tf_op jit(solution)/shard_map/dot_general | solution.py:125
  (15 shorter events, 0.0 us)
Async XLA Ops:
  7.2 80.7 %copy-start.6 = (f32[256]{0:T(256)S(1)}, f32[256]{0:T(256)}, u32[]{:S(2)}) copy-start(f32[256]{0:T(256)} %param.19) | copy-start | bytes 3076
  7.2 77.5 %all-gather.3.cloned.1.call-start = ((), (), s32[]{:S(2)}) async-start(), calls=%async_computation.1 | async-start | bytes 8912896 | tf_op jit(solution)/shard_map/all_gather | solution.py:15
  9.2 180.9 %all-gather.5.cloned.1.call-start = ((), (), s32[]{:S(2)}) async-start(), calls=%async_computation.2 | async-start | bytes 2621440 | tf_op jit(solution)/shard_map/all_gather | solution.py:43
  22.6 66.8 %copy-start.1 = (bf16[256,4096]{1,0:T(8,128)(2,1)S(1)}, bf16[256,4096]{1,0:T(8,128)(2,1)}, u32[]{:S(2)}) copy-start(bf16[256,4096]{1,0:T(8,128)(2,1)} %param.13) | copy-start | bytes 6291460
  22.6 66.8 %copy-start.7 = (f32[4096]{0:T(1024)S(1)}, f32[4096]{0:T(1024)}, u32[]{:S(2)}) copy-start(f32[4096]{0:T(1024)} %param.14) | copy-start | bytes 49156
  100.6 19.9 %copy-start.5 = (f32[64,2,128]{2,1,0:T(2,128)S(1)}, f32[64,2,128]{2,1,0:T(2,128)}, u32[]{:S(2)}) copy-start(f32[64,2,128]{2,1,0:T(2,128)} %get-tuple-element.25) | copy-start | bytes 196612
  120.4 36.6 %copy-start = (f32[64,2,128,128]{3,2,1,0:T(8,128)}, f32[64,2,128,128]{3,2,1,0:T(8,128)S(1)}, u32[]{:S(2)}) copy-start(f32[64,2,128,128]{3,2,1,0:T(8,128)S(1)} %multiply_add_fusion.3) | copy-start | bytes 25165828
  120.5 11.7 %copy-start.4 = (f32[64,2,128]{2,1,0:T(2,128)S(1)}, f32[64,2,128]{2,1,0:T(2,128)}, u32[]{:S(2)}) copy-start(f32[64,2,128]{2,1,0:T(2,128)} %get-tuple-element.24) | copy-start | bytes 196612
  151.1 5.9 %copy-start.2 = (f32[64,2,128]{2,0,1:T(8,128)S(1)}, f32[64,2,128]{2,0,1:T(8,128)}, u32[]{:S(2)}) copy-start(f32[64,2,128]{2,0,1:T(8,128)} %get-tuple-element.15) | copy-start | bytes 196612
  151.1 5.9 %copy-start.3 = (f32[64,2,128]{2,1,0:T(2,128)S(1)}, f32[64,2,128]{2,1,0:T(2,128)}, u32[]{:S(2)}) copy-start(f32[64,2,128]{2,1,0:T(2,128)} %get-tuple-element.23) | copy-start | bytes 196612
  157.0 24.4 %copy-start.8 = (f32[4096]{0:T(1024)S(1)}, f32[4096]{0:T(1024)}, u32[]{:S(2)}) copy-start(f32[4096]{0:T(1024)} %param.14) | copy-start | bytes 49156
  157.1 24.4 %copy-start.9 = (f32[256]{0:T(256)S(1)}, f32[256]{0:T(256)}, u32[]{:S(2)}) copy-start(f32[256]{0:T(256)} %param.20) | copy-start | bytes 3076
  185.0 20.1 %all-to-all-start = ((bf16[8,256,256]{1,2,0:T(8,128)(2,1)}), bf16[8,256,256]{1,2,0:T(8,128)(2,1)S(1)}, u32[]{:S(2)}, u32[]{:S(2)}) async-start(bf16[8,256,256]{1,2,0:T(8,128)(2,1)} %broadcast_in_dim.60), calls=%async_computation | async-start | bytes 2097152 | tf_op jit(solution)/shard_map/all_to_all | solution.py:24
Sparse Core Ops, SparseCore 0:
  10.7 73.9 all-gather.2
  86.4 30.5 all-gather.4
where the time goes:
time: 215 us
  matrix products  74.3 us (35%)
  waiting for transfers between devices  71 us (33%)
  other arithmetic  27.6 us (13%)
  between operations  14.4 us (7%)
  blocking collectives  13.3 us (6%)
  local copies, waits for them, and re-layouts  9.11 us (4%)
  starting transfers between devices  5.19 us (2%)
    dot_general x4, matrix products, recur_one(): outputs.append(jnp.einsum('hd,hde->he', queries[position], carried))  59.7 us
    all_gather x1, waiting for transfers between devices, in_one_piece(): lax.all_gather(both, axis, axis=dim, tiled=True)  56 us
    add x1, other arithmetic, recur_one(): decay_rate[:, :, None] * carried  19.9 us
    all_to_all x1, waiting for transfers between devices, sent_to_all(): lax.all_to_all(jnp.broadcast_to(array[None], (size, *array.shape)), axis,...  15 us
    all_gather x1, blocking collectives, gathered_by_axis(): nearer = lax.all_gather(array, axes[-1], axis=dim, tiled=True)  13.3 us
    dot_general x4, matrix products, on_device(): jnp.dot(columns, weight_piece, preferred_element_type=jnp.float32)  11.6 us
    all_to_all x1, starting transfers between devices, sent_to_all(): lax.all_to_all(jnp.broadcast_to(array[None], (size, *array.shape)), axis,...  5.11 us
  transfers between devices with their start and end apart: 3, of which 2 were waited for; matrix products, arithmetic and copies ran while one was open for 49% of the time, Pallas kernels for 0%

commit v1 on v0

v1 whole, which is shorter than its diff:
```python
import functools
import heapq

import jax
import jax.numpy as jnp
from jax import lax
from jax.experimental import pallas as pl
from jax.experimental.pallas import tpu as pltpu
from jax.sharding import Mesh
from jax.sharding import PartitionSpec as P

EPSILON = 1e-06
MESH = pl.DeviceIdType.MESH
F32, BF16 = jnp.float32, jnp.bfloat16

FIRST = ("y", "y", "z", "z")
SIGN = (1, -1, 1, -1)
OTHER = {"y": "z", "z": "y"}


def forwards(u, a, b):
    first, second, sign = FIRST[u], OTHER[FIRST[u]], SIGN[u]
    if b == 0:
        go = [(second, sign), (second, -sign)]
        if a == 0:
            return [(first, sign), (first, -sign)] + go
        if a == (-sign) % 4:
            return [(first, sign)] + go
        return go
    return [(second, sign)] if b == (-sign) % 4 else []


def lands_at(u, a, b, axis, way):
    if axis == FIRST[u]:
        return (a - way) % 4, b
    return a, (b - way) % 4


@functools.cache
def arrival_order(wire=2.8, delay=2.0):
    free, events, count = {}, [], 0

    def send(now, u, a, b, axis, way):
        nonlocal count
        end = max(now, free.get((axis, way), 0.0)) + wire
        free[axis, way] = end
        count += 1
        heapq.heappush(events, (end + delay, count, u, *lands_at(u, a, b, axis, way)))

    own = [(u, *go) for u in range(4) for go in forwards(u, 0, 0)]
    own.sort(key=lambda item: item[1] != FIRST[item[0]])
    for u, axis, way in own:
        send(0.0, u, 0, 0, axis, way)
    order = []
    while events:
        now, _, u, a, b = heapq.heappop(events)
        order.append((u, a, b))
        for axis, way in forwards(u, a, b):
            send(now, u, a, b, axis, way)
    return tuple(own), tuple(order)


def spot(u, a, b):
    return u * 16 + a * 4 + b


def gate_of(pre_act, bound):
    return bound + (1.0 - bound) * jax.nn.sigmoid(pre_act)


def taken_kernel(forget_ref, value_ref, bound_ref, accepted_ref, state_ref, taken_ref):
    seqs = state_ref.shape[0]
    count = accepted_ref[...]
    bound = bound_ref[...]
    gates, keys = [], []
    for t in range(4):
        kept = t < count
        g = gate_of(forget_ref[:, t, :].astype(F32), bound)
        gates.append(jnp.where(kept, g, 1.0))
        keys.append(jnp.where(kept, 1.0 - g, 0.0))
    after = jnp.ones_like(gates[0])
    weights = [None] * 4
    for t in (3, 2, 1, 0):
        weights[t] = keys[t] * after
        after = after * gates[t]

    def two_parts(x):
        high = x.astype(BF16).astype(F32)
        return high, x - high

    parts = [two_parts(w) for w in weights]
    whole = two_parts(after)
    rows = [p[0] for p in parts] + [p[1] for p in parts] + [whole[0], whole[1]]
    left = jnp.concatenate(rows, axis=0)
    values = jnp.concatenate([value_ref[:, t, :].astype(F32) for t in range(4)] * 2, axis=0)
    height = 10 * seqs
    values = jnp.concatenate([values, jnp.zeros((2 * seqs, values.shape[1]), F32)], axis=0)
    row = lax.broadcasted_iota(jnp.int32, (height, 128), 0)
    for h in range(2):
        lanes = slice(128 * h, 128 * h + 128)
        v = values[:, lanes]
        right = []
        for j in range(seqs):
            mine = row % seqs == j
            right.append(jnp.where(mine, v, 0.0))
            right.append(jnp.where(mine & (row >= 8 * seqs), 1.0, 0.0))
        right = jnp.concatenate(right, axis=1).astype(BF16)
        both = lax.dot_general(
            left[:, lanes].astype(BF16), right, (((0,), (0,)), ((), ())), preferred_element_type=F32
        )
        for j in range(seqs):
            added = both[:, 256 * j : 256 * j + 128]
            decay = both[:, 256 * j + 128 : 256 * j + 256]
            taken_ref[j, h] = state_ref[j, h] * decay + added


def taken_of(prev_forget, prev_value, lower_bound, accepted, state):
    seqs, per = state.shape[0], 8
    return pl.pallas_call(
        taken_kernel,
        grid=(seqs // per,),
        in_specs=[
            pl.BlockSpec((per, 4, 256), lambda i: (i, 0, 0)),
            pl.BlockSpec((per, 4, 256), lambda i: (i, 0, 0)),
            pl.BlockSpec((1, 256), lambda i: (0, 0)),
            pl.BlockSpec((per, 1), lambda i: (i, 0)),
            pl.BlockSpec((per, 2, 128, 128), lambda i: (i, 0, 0, 0)),
        ],
        out_specs=pl.BlockSpec((per, 2, 128, 128), lambda i: (i, 0, 0, 0)),
        out_shape=jax.ShapeDtypeStruct(state.shape, F32),
        name="taken_state",
    )(prev_forget, prev_value, lower_bound.reshape(1, 256), accepted.reshape(seqs, 1), state)


def layer_kernel(
    tokens, gain, w0, w1, w2, w3, bound, head_gain, w_out, taken,
    mixed,
    raw, normed, gathered, sums, out_weights, halves, packed, heads, queries, rest,
    send_sem, wide_recv, out_recv, out_send, head_send, head_recv, relay_recv, local_sem, state_sem,
):
    z, y, x, c = (lax.axis_index(name) for name in ("z", "y", "x", "c"))
    here = {"z": z, "y": y}
    mine = z * 4 + y
    me = x * 2 + c
    weights = (w0, w1, w2, w3)

    barrier = pltpu.get_barrier_semaphore()
    partners = [{axis: (here[axis] + way) % 4} for axis in ("y", "z") for way in (1, 3)]
    partners += [{"x": (x + way) % 4} for way in (1, 2, 3)] + [{"c": 1 - c}]
    for partner in partners:
        pl.semaphore_signal(barrier, inc=1, device_id=partner, device_id_type=MESH)

    token_copy = pltpu.make_async_copy(tokens, raw, local_sem.at[0])
    token_copy.start()
    own_copies = [
        pltpu.make_async_copy(weights[u], gathered.at[u, mine], local_sem.at[1 + u]) for u in range(4)
    ]
    own_copies.append(pltpu.make_async_copy(w_out, out_weights.at[mine], local_sem.at[5]))
    for copy in own_copies:
        copy.start()

    def state_copy(i):
        return pltpu.make_async_copy(
            taken.at[pl.ds(8 * i, 8)], halves.at[i % 2], state_sem.at[i % 2]
        )

    state_copy(0).start()
    state_copy(1).start()
    pl.semaphore_wait(barrier, len(partners))

    def owner(u, a, b):
        at = {FIRST[u]: a, OTHER[FIRST[u]]: b}
        return (z + at["z"]) % 4 * 4 + (y + at["y"]) % 4

    def wide(u, a, b, axis, way):
        k = owner(u, a, b)
        return pltpu.make_async_remote_copy(
            src_ref=weights[u] if a == b == 0 else gathered.at[u, k],
            dst_ref=gathered.at[u, k],
            send_sem=send_sem,
            recv_sem=wide_recv.at[spot(u, *lands_at(u, a, b, axis, way))],
            device_id={axis: (here[axis] + way) % 4},
            device_id_type=MESH,
        )

    def wide_arrival(u, a, b):
        k = owner(u, a, b)
        pltpu.make_async_copy(gathered.at[u, k], gathered.at[u, k], wide_recv.at[spot(u, a, b)]).wait()

    def slim(u, a, b, axis, way):
        k = owner(u, a, b)
        rows = pl.ds(32 * u, 32)
        return pltpu.make_async_remote_copy(
            src_ref=w_out.at[rows] if a == b == 0 else out_weights.at[k, rows],
            dst_ref=out_weights.at[k, rows],
            send_sem=out_send,
            recv_sem=out_recv.at[spot(u, *lands_at(u, a, b, axis, way))],
            device_id={axis: (here[axis] + way) % 4},
            device_id_type=MESH,
        )

    def slim_arrival(u, a, b):
        part = out_weights.at[owner(u, a, b), pl.ds(32 * u, 32)]
        pltpu.make_async_copy(part, part, out_recv.at[spot(u, a, b)]).wait()

    own, order = arrival_order()
    for u, axis, way in own:
        wide(u, 0, 0, axis, way).start()

    token_copy.wait()

    @pl.loop(0, 16)
    def _(i):
        rows = pl.ds(pl.multiple_of(16 * i, 16), 16)
        floated = raw[rows, :].astype(F32)
        scale = lax.rsqrt(jnp.mean(floated * floated, axis=-1, keepdims=True) + EPSILON)
        scaled = (floated * scale * gain[...]).astype(BF16)
        for k in range(16):
            normed[k, rows, :] = scaled[:, 256 * k : 256 * k + 256]

    def add_product(u, k, first=False):
        product = jnp.dot(normed[k], gathered[u, k], preferred_element_type=F32)
        sums[u] = product if first else sums[u] + product

    def pack_state(i):
        state_copy(i).wait()

        @pl.loop(0, 8)
        def _(j):
            packed[8 * i + j] = halves[i % 2, j].astype(BF16)

        if i + 2 < 8:
            state_copy(i + 2).start()

    for copy in own_copies:
        copy.wait()
    for u in range(4):
        add_product(u, mine, first=True)

    for n, (u, a, b) in enumerate(order):
        wide_arrival(u, a, b)
        for axis, way in forwards(u, a, b):
            wide(u, a, b, axis, way).start()
        if n == 47:
            for v, axis, way in own:
                slim(v, 0, 0, axis, way).start()
        add_product(u, owner(u, a, b))
        if n % 4 == 3 and n // 4 < 8:
            pack_state(n // 4)

    def slim_steps(at):
        for u, a, b in order[15 * at : 15 * at + 15]:
            slim_arrival(u, a, b)
            for axis, way in forwards(u, a, b):
                slim(u, a, b, axis, way).start()

    row = lax.broadcasted_iota(jnp.int32, (64, 128), 0)
    step = row % 4
    row16 = lax.broadcasted_iota(jnp.int32, (16, 128), 0)

    def head_copy(block, to):
        part = heads.at[me, pl.ds(64 * block, 64)]
        if to == 0:
            where, sem = {"c": 1 - c}, relay_recv.at[block]
        else:
            where, sem = {"x": (x + to) % 4}, head_recv.at[4 * to + block]
        return pltpu.make_async_remote_copy(
            src_ref=part, dst_ref=part, send_sem=head_send, recv_sem=sem,
            device_id=where, device_id_type=MESH,
        )

    for block in range(4):
        rows = slice(64 * block, 64 * block + 64)
        for h in range(2):
            lanes = slice(128 * h, 128 * h + 128)
            q, p, v, gate = (
                sums[u, rows, lanes].astype(BF16).astype(F32) for u in range(4)
            )
            q = q * 128 ** -0.5
            g = gate_of(p, bound[:, lanes])
            k = 1.0 - g
            decay = g
            total = jnp.sum(q * k, axis=-1, keepdims=True) * v
            reach = jnp.where(step == 0, g, 0.0)
            for lag in (1, 2, 3):
                score = jnp.sum(q * decay * pltpu.roll(k, lag, 0), axis=-1, keepdims=True)
                total = total + jnp.where(step >= lag, score * pltpu.roll(v, lag, 0), 0.0)
                decay = decay * pltpu.roll(g, lag, 0)
                reach = jnp.where(step == lag, decay, reach)
            queries[...] = (q * reach).astype(BF16)
            rest[...] = total
            for four in range(4):
                part = slice(16 * four, 16 * four + 16)
                lhs = queries[part]
                found = rest[part]
                for j in range(4):
                    seq = 16 * block + 4 * four + j
                    product = jnp.dot(lhs, packed[seq, h], preferred_element_type=F32)
                    found = found + jnp.where(row16 // 4 == j, product, 0.0)
                rest[part] = found
            total = rest[...]
            scaled = total * lax.rsqrt(jnp.mean(total * total, axis=-1, keepdims=True) + EPSILON)
            heads[me, rows, lanes] = (
                scaled * head_gain[:, lanes] * (gate * jax.nn.sigmoid(gate))
            ).astype(BF16)
        for to in (0, 1, 3, 2):
            head_copy(block, to).start()
        slim_steps(block)

    def relay(block, to, where):
        part = heads.at[(x - to) % 4 * 2 + where, pl.ds(64 * block, 64)]
        return pltpu.make_async_remote_copy(
            src_ref=part, dst_ref=part, send_sem=head_send, recv_sem=relay_recv.at[4 * to + block],
            device_id={"c": 1 - c}, device_id_type=MESH,
        )

    for block in range(4):
        for to in (1, 3, 2):
            part = heads.at[(x - to) % 4 * 2 + c, pl.ds(64 * block, 64)]
            pltpu.make_async_copy(part, part, head_recv.at[4 * to + block]).wait()
            relay(block, to, c).start()
    for to in (0, 1, 3, 2):
        for block in range(4):
            relay(block, to, 1 - c).wait_recv()

    for half in range(2):
        rows = slice(128 * half, 128 * half + 128)
        total = jnp.zeros((128, 512), F32)
        for t in range(8):
            weight = out_weights[2 * t : 2 * t + 2].reshape(256, 512)
            total = total + jnp.dot(heads[t, rows], weight, preferred_element_type=F32)
        mixed[rows] = total.astype(BF16)

    sent = gathered.at[:, pl.ds(0, 15)]
    pltpu.make_async_copy(sent, sent, send_sem).wait()
    sent = out_weights.at[pl.ds(0, 15)]
    pltpu.make_async_copy(sent, sent, out_send).wait()
    sent = heads.at[pl.ds(0, 7)]
    pltpu.make_async_copy(sent, sent, head_send).wait()


def layer_of(tokens, gain, weights, bound, head_gain, w_out, taken):
    anywhere = pl.BlockSpec(memory_space=pl.ANY)
    inside = pl.BlockSpec(memory_space=pltpu.VMEM)
    return pl.pallas_call(
        layer_kernel,
        in_specs=[anywhere, inside] + [anywhere] * 4 + [inside, inside, anywhere, anywhere],
        out_specs=inside,
        out_shape=jax.ShapeDtypeStruct((256, 512), BF16),
        scratch_shapes=[
            pltpu.VMEM((256, 4096), BF16),
            pltpu.VMEM((16, 256, 256), BF16),
            pltpu.VMEM((4, 16, 256, 256), BF16),
            pltpu.VMEM((4, 256, 256), F32),
            pltpu.VMEM((16, 128, 512), BF16),
            pltpu.VMEM((2, 8, 2, 128, 128), F32),
            pltpu.VMEM((64, 2, 128, 128), BF16),
            pltpu.VMEM((8, 256, 256), BF16),
            pltpu.VMEM((64, 128), BF16),
            pltpu.VMEM((64, 128), F32),
            pltpu.SemaphoreType.DMA,
            pltpu.SemaphoreType.DMA((64,)),
            pltpu.SemaphoreType.DMA((64,)),
            pltpu.SemaphoreType.DMA,
            pltpu.SemaphoreType.DMA,
            pltpu.SemaphoreType.DMA((16,)),
            pltpu.SemaphoreType.DMA((16,)),
            pltpu.SemaphoreType.DMA((6,)),
            pltpu.SemaphoreType.DMA((2,)),
        ],
        compiler_params=pltpu.CompilerParams(collective_id=0, has_side_effects=True),
        name="layer",
    )(tokens, gain.reshape(1, 4096), *weights, bound.reshape(1, 256), head_gain.reshape(1, 256), w_out, taken)


def on_device(
    tokens, norm_gain, w_query, w_forget, w_value, w_gate, lower_bound, head_gain, w_out,
    state, prev_forget, prev_value, accepted,
):
    taken = taken_of(prev_forget, prev_value, lower_bound, accepted, state)
    mixed = layer_of(
        tokens, norm_gain, (w_query, w_forget, w_value, w_gate), lower_bound, head_gain, w_out, taken
    )
    return mixed, taken


def solution(mesh):
    finer = Mesh(mesh.devices.reshape(4, 4, 4, 2), ("z", "y", "x", "c"))
    kv, tp = ("z", "y"), ("x", "c")
    placed = (
        P(kv, None), P(), P(kv, tp), P(kv, tp), P(kv, tp), P(kv, tp), P(tp), P(tp), P(kv, tp),
        P(kv, tp, None, None), P(kv, None, tp), P(kv, None, tp), P(kv),
    )
    return jax.shard_map(
        on_device, mesh=finer, in_specs=placed,
        out_specs=(P(kv, tp), P(kv, tp, None, None)), check_vma=False,
    )
```

time: 215 us -> 88.1 us (0.41)
  Pallas kernels: 0 us -> 84.1 us
  matrix products: 74.3 us -> 0 us
  waiting for transfers between devices: 71 us -> 0 us
  other arithmetic: 27.6 us -> 0 us
  between operations: 14.4 us -> 0.64 us
  blocking collectives: 13.3 us -> 0 us
  local copies, waits for them, and re-layouts: 9.11 us -> 3.03 us
  starting transfers between devices: 5.19 us -> 0 us
    pallas_call x0 -> x2, Pallas kernels: none -> 84.1 us  [the longest x1 73 us: layer_of(): pl.pallas_call(layer_kernel, in_specs=[anywhere, inside] + [anywhere] * 4...]
    dot_general x9 -> x0, matrix products: 74.3 us -> none  [the longest x4 59.7 us: recur_one(): outputs.append(jnp.einsum('hd,hde->he', queries[position], carried))]
    all_gather x2 -> x0, waiting for transfers between devices: 56 us -> none  [the longest x1 56 us: in_one_piece(): lax.all_gather(both, axis, axis=dim, tiled=True)]
    add x2 -> x0, other arithmetic: 19.9 us -> none  [the longest x1 19.9 us: recur_one(): decay_rate[:, :, None] * carried]
    all_to_all x1 -> x0, waiting for transfers between devices: 15 us -> none  [sent_to_all(): lax.all_to_all(jnp.broadcast_to(array[None], (size, *array.shape)), axis,...]
    all_gather x1 -> x0, blocking collectives: 13.3 us -> none  [gathered_by_axis(): nearer = lax.all_gather(array, axes[-1], axis=dim, tiled=True)]
    all_to_all x1 -> x0, starting transfers between devices: 5.11 us -> none  [sent_to_all(): lax.all_to_all(jnp.broadcast_to(array[None], (size, *array.shape)), axis,...]
    mul x8 -> x0, local copies, waits for them, and re-layouts: 4.48 us -> none  [the longest x5 2.56 us: recur_one(): forget[position][:, :, None] * carried]
  transfers between devices with their start and end apart: 3 -> 0, of which waited for: 2 -> 0; matrix products, arithmetic and copies ran while one was open for 49% -> 0% of each run, Pallas kernels for 0% -> 0%
where the time goes in v1:
time: 88.1 us; the launch traced here: 87.8 us
  Pallas kernels  84.1 us (95%)
  local copies, waits for them, and re-layouts  3.03 us (3%)
    pallas_call x1, Pallas kernels, layer_of(): pl.pallas_call(layer_kernel, in_specs=[anywhere, inside] + [anywhere] * 4...  73 us
    pallas_call x1, Pallas kernels, taken_of(): pl.pallas_call(taken_kernel, grid=(seqs // per,), in_specs=[pl.BlockSpec(...  11.1 us

profile of v1, /device:TPU:1, one launch (start us, length us, event | category | flops | bytes accessed | tf_op | source)
XLA Modules:
  0.0 87.8 jit_solution(8179627254213163822)
XLA Ops:
  0.6 1.4 %copy.15.accepted_ref = s32[64,1]{1,0:T(8,128)} copy(s32[64,1]{0,1:T(1,128)} %bitcast.8) | data formatting | bytes 512 | tf_op jit(solution)/shard_map/reshape | solution.py:132
  2.0 11.1 %taken_state.1.taken = f32[64,2,128,128]{3,2,1,0:T(8,128)} custom-call(bf16[64,4,256]{2,1,0:T(4,128)(2,1)} %forget_ref.1, bf16[64,4,256]{2,1,0:T(4,128)(2,1)} %value_ref.1, f32[1,256]{1,0:T(1,128)} %bitcast.5, s32[64,1]{1,0:T(8,128)} %copy.15.accepted_ref, f32[64,2,128,128]{3,2,1,0:T(8,128)} %state_ref.1), custom_call_target="tpu_custom_call" | custom-call | tf_op jit(solution)/shard_map/taken_state/pallas_call | solution.py:119
  13.1 73.0 %layer.1 = bf16[256,512]{1,0:T(8,128)(2,1)} custom-call(bf16[256,4096]{1,0:T(8,128)(2,1)} %tokens.1, f32[1,4096]{1,0:T(1,128)} %bitcast.4, bf16[256,256]{1,0:T(8,128)(2,1)} %w0.1, bf16[256,256]{1,0:T(8,128)(2,1)} %w1.1, bf16[256,256]{1,0:T(8,128)(2,1)} %w2.1, bf16[256,256]{1,0:T(8,128)(2,1)} %w3.1, f32[1,256]{1,0:T(1,128)} %bitcast.6, f32[1,256]{1,0:T(1,128)} %bitcast.7, ...), custom_call_target="tpu_custom_call" | custom-call | tf_op jit(solution)/shard_map/layer/pallas_call | solution.py:345
  86.1 1.7 %copy.17 = bf16[256,512]{1,0:T(8,128)(2,1)} copy(bf16[256,512]{1,0:T(8,128)(2,1)} %layer.1) | data formatting | bytes 524288

commit v2 on v0

v2 whole, which is shorter than its diff:
```python
import functools
import heapq

import jax
import jax.numpy as jnp
from jax import lax
from jax.experimental import pallas as pl
from jax.experimental.pallas import tpu as pltpu
from jax.sharding import Mesh
from jax.sharding import PartitionSpec as P

EPSILON = 1e-06
MESH = pl.DeviceIdType.MESH
F32, BF16 = jnp.float32, jnp.bfloat16

SIGN = ("z+", "z-", "z+", "z-")


def shifted(dz, link):
    return {"z+": (dz - 1) % 4, "z-": (dz + 1) % 4}.get(link, dz)


def sends(item):
    kind = item[0]
    if kind == "w":
        _, u, s, dz, dy = item
        way = SIGN[u]
        other = "z-" if way == "z+" else "z+"
        links = []
        if u < 2:
            if dy == 0:
                if dz == 0:
                    links = [way, other]
                elif dz == (3 if way == "z+" else 1):
                    links = [way]
                links = links + ["yi"]
        else:
            if dz == 0:
                links = (["yi"] if dy == 0 else []) + [way, other]
            elif dz == (3 if way == "z+" else 1):
                links = [way]
        return [(k, ("w", u, s, shifted(dz, k), 1 if k == "yi" else dy)) for k in links]
    if kind == "o":
        _, u, dz, dy = item
        way = SIGN[u]
        other = "z-" if way == "z+" else "z+"
        along_y = {0: ["yi", "yo"], 1: ["yo"]}.get(dy, [])
        along_z = [way, other] if dz == 0 else [way] if dz == (3 if way == "z+" else 1) else []
        if u < 2:
            links = along_y + along_z if dz == 0 else along_z
        else:
            links = along_z + along_y if dy == 0 else along_y
        turned = {("yi", 0): 1, ("yo", 0): 3, ("yo", 1): 2}
        return [(k, ("o", u, shifted(dz, k), turned.get((k, dy), dy))) for k in links]
    if kind in "th":
        at, b = item[-2], item[-1]
        first, over = item[:-2], {"t": "u", "h": "g"}[kind]
        go = [("c", (over, *first[1:], at, b))]
        if at == 0:
            go = [("x+", (*first, 1, b)), ("x-", (*first, 2, b))] + go
        elif at == 1 and b % 2 == 0:
            go = [("x+", (*first, 3, b))] + go
        elif at == 2 and b % 2 == 1:
            go = [("x-", (*first, 3, b))] + go
        return go
    return []


SIZE = {"w": 64, "o": 32, "t": 128, "u": 128, "h": 16, "g": 16, "q": 64}
OUT_AT = 20
TIMES = {"norm": 2.2, "norm2": 2.2, "take": 1.4, "product": 0.17, "away": 0.15, "recur": 0.4}


@functools.cache
def plan():
    free, events, steps = {}, [], []
    now, count, arrived_w, out_started = 0.0, 0, 0, False
    done, ready = set(), []
    work = [("norm",)] + [("take", i) for i in range(8)]
    products = [(u, 0, 0, 0) for u in range(4)]
    stage = {"tokens": 0, "products": 0, "recur": 0}

    def send(item, link, there):
        nonlocal count
        begin = max(now, free.get(link, 0.0))
        rate = 0.0017 if link == "c" else 0.0215
        free[link] = begin + SIZE[item[0]] * rate
        count += 1
        heapq.heappush(events, (free[link] + (1.0 if link == "c" else 2.2), count, there))
        steps.append(("start", item, link, there))

    def go_on(item):
        for link, there in sends(item):
            send(item, link, there)

    own = [("w", u, 0, 0, 0) for u in range(4)]
    for u in (0, 2, 1, 3):
        send(("w", u, 1, None, None), "yo", ("w", u, 1, 0, 0))
        if u in (0, 1):
            send(("t", 0, u), "yo", ("t", 0, u))
    for item in own:
        go_on(item)

    def task():
        if work and work[0][0] == "norm":
            return work.pop(0)
        if stage["tokens"] == 16:
            stage["tokens"] = 0
            stage["ready"] = 1
            return ("norm2",)
        if "ready" in stage and products:
            stage["products"] += 1
            if stage["products"] == 64:
                work.extend([("away", b) for b in range(4)] + [("recur", 0, b) for b in range(4)])
            return ("product", *products.pop(0))
        return work.pop(0) if work else None

    while True:
        if events and events[0][0] <= now:
            _, _, item = heapq.heappop(events)
            steps.append(("wait", item))
            go_on(item)
            if item[0] == "w":
                products.append(item[1:])
                arrived_w += 1
                if arrived_w == OUT_AT:
                    for u in range(4):
                        go_on(("o", u, 0, 0))
            elif item[0] in "tu":
                stage["tokens"] += 1
            elif item[0] == "q":
                work.append(("recur", 1, item[1]))
            now += 0.02
            continue
        job = task()
        if job is not None:
            steps.append(job)
            now += TIMES[job[0]]
            if job[0] == "away":
                send(("q", job[1]), "yo", ("q", job[1]))
            elif job[0] == "recur":
                go_on(("h", job[1], 0, job[2]))
        elif events:
            now = events[0][0]
        else:
            return tuple(steps), now


def gate_of(pre_act, bound):
    return bound + (1.0 - bound) * jax.nn.sigmoid(pre_act)


def two_parts(x):
    high = x.astype(BF16).astype(F32)
    return high, x - high


def layer_kernel(
    accepted_in, tokens, gain_in, w0, w1, w2, w3, bound_in, head_gain_in, w_out, state, forget_in, value_in,
    taken, heads, out_weights,
    raw, raw_more, normed, gathered, sums, away, given, packed, queries, rest,
    gain, bound, head_gain, old_forget, old_value, accepted,
    send_sem, out_send, head_send, token_send, given_send,
    w_recv, o_recv, t_recv, h_recv, q_recv, local_sem, state_sem,
):
    z, y, x, c = (lax.axis_index(name) for name in ("z", "y", "x", "c"))
    inner, outer = y + 1 - 2 * (y % 2), 3 - y
    mine = z * 4 + y
    me = x * 2 + c
    head = y // 2
    weights = (w0, w1, w2, w3)
    target = {
        "z+": {"z": (z + 1) % 4}, "z-": {"z": (z + 3) % 4}, "yi": {"y": inner}, "yo": {"y": outer},
        "x+": {"x": (x + 1) % 4}, "x-": {"x": (x + 3) % 4}, "c": {"c": 1 - c},
    }

    barrier = pltpu.get_barrier_semaphore()
    for partner in target.values():
        pl.semaphore_signal(barrier, inc=1, device_id=partner, device_id_type=MESH)

    def columns(h):
        return pl.ds(pl.multiple_of(128 * h, 128), 128)

    token_copies = [
        pltpu.make_async_copy(tokens, raw, local_sem.at[0]),
        pltpu.make_async_copy(gain_in, gain, local_sem.at[1]),
    ]
    small_copies = [
        pltpu.make_async_copy(bound_in, bound, local_sem.at[2]),
        pltpu.make_async_copy(head_gain_in, head_gain, local_sem.at[3]),
        pltpu.make_async_copy(forget_in, old_forget, local_sem.at[4]),
        pltpu.make_async_copy(value_in, old_value, local_sem.at[5]),
        pltpu.make_async_copy(accepted_in, accepted, local_sem.at[11]),
    ]
    own_copies = [
        pltpu.make_async_copy(weights[u].at[:, columns(head)], gathered.at[u, mine], local_sem.at[6 + u])
        for u in range(4)
    ]
    own_copies.append(pltpu.make_async_copy(w_out, out_weights.at[mine], local_sem.at[10]))

    def state_copy(i):
        part = pl.ds(8 * i, 8)
        return pltpu.make_async_copy(state.at[part], taken.at[part], state_sem.at[i])

    for copy in token_copies + own_copies + small_copies:
        copy.start()
    for i in range(8):
        state_copy(i).start()
    pl.semaphore_wait(barrier, len(target))

    def chip(kind):
        return (x + (0, 3, 1, 2)[kind]) % 4

    def place(item, core):
        kind = item[0]
        if kind == "w":
            _, u, s, dz, dy = item
            row = y if dy == 0 else inner
            return gathered.at[u, (z + dz) % 4 * 4 + (3 - row if s else row)]
        if kind == "o":
            _, u, dz, dy = item
            row = (y, inner, (y + 2) % 4, outer)[dy]
            return out_weights.at[(z + dz) % 4 * 4 + row, pl.ds(32 * u, 32)]
        if kind in "tu":
            _, at, part = item
            return raw_more.at[chip(at) * 2 + core, pl.ds(16 * part, 16)]
        if kind in "hg":
            _, n, at, b = item
            which = (chip(at) * 2 + core) * 2 + (1 - head if n else head)
            return heads.at[which, pl.ds(64 * b, 64)]
        return given.at[item[1]]

    def arrival(item):
        kind = item[0]
        if kind == "w":
            _, u, s, dz, dy = item
            return w_recv.at[u * 16 + s * 8 + dz * 2 + dy]
        if kind == "o":
            _, u, dz, dy = item
            return o_recv.at[u * 16 + dz * 4 + dy]
        if kind in "tu":
            return t_recv.at[(8 if kind == "u" else 0) + item[1] * 2 + item[2]]
        if kind in "hg":
            _, n, at, b = item
            return h_recv.at[(32 if kind == "g" else 0) + n * 16 + at * 4 + b]
        return q_recv.at[item[1]]

    leaving = {"w": send_sem, "o": out_send, "t": token_send, "h": head_send, "q": given_send}

    def start(item, link, there):
        kind = item[0]
        if kind == "w" and item[3] is None:
            source, to = weights[item[1]].at[:, columns(1 - head)], gathered.at[item[1], mine]
        elif kind == "w" and item[2:] == (0, 0, 0):
            source, to = weights[item[1]].at[:, columns(head)], gathered.at[item[1], mine]
        elif kind == "o" and item[2:] == (0, 0):
            source, to = w_out.at[pl.ds(32 * item[1], 32)], place(item, c)
        elif kind == "t" and link == "yo":
            rows = pl.ds(pl.multiple_of(32 * me + 16 * item[2], 16), 16)
            source, to = tokens.at[rows], place(item, c)
        elif kind == "q":
            source, to = away.at[item[1]], given.at[item[1]]
        else:
            source = to = place(item, c)
        pltpu.make_async_remote_copy(
            src_ref=source, dst_ref=to, send_sem=leaving[kind], recv_sem=arrival(there),
            device_id=target[link], device_id_type=MESH,
        ).start()

    def wait(item):
        ref = place(item, 1 - c if item[0] in "ug" else c)
        pltpu.make_async_copy(ref, ref, arrival(item)).wait()

    def normalize(take_rows, first):
        @pl.loop(0, 16)
        def _(i):
            floated = take_rows(i).astype(F32)
            scale = lax.rsqrt(jnp.mean(floated * floated, axis=-1, keepdims=True) + EPSILON)
            scaled = (floated * scale * gain[...]).astype(BF16)
            rows = pl.ds(pl.multiple_of(first + 16 * i, 16), 16)
            for k in range(16):
                normed[k, rows, :] = scaled[:, 256 * k : 256 * k + 256]

    def norm():
        for copy in token_copies:
            copy.wait()
        normalize(lambda i: raw[pl.ds(pl.multiple_of(16 * i, 16), 16), :], 0)
        for copy in own_copies + small_copies:
            copy.wait()

    def norm2():
        normalize(lambda i: raw_more[i // 2, pl.ds(pl.multiple_of(i % 2 * 16, 16), 16), :], 256)

    begun = set()

    def product(u, s, dz, dy):
        row = y if dy == 0 else inner
        k = (z + dz) % 4 * 4 + (3 - row if s else row)
        found = jnp.dot(normed[k], gathered[u, k], preferred_element_type=F32)
        sums[u] = sums[u] + found if u in begun else found
        begun.add(u)

    row8 = lax.broadcasted_iota(jnp.int32, (8, 256), 0)
    row80 = lax.broadcasted_iota(jnp.int32, (80, 128), 0)

    def take(i):
        state_copy(i).wait()
        seqs = pl.ds(pl.multiple_of(8 * i, 8), 8)
        count = jnp.zeros((8, 256), jnp.int32)
        for j in range(8):
            count = jnp.where(row8 == j, accepted[8 * i + j], count)
        gates, keys = [], []
        for t in range(4):
            g = gate_of(old_forget[seqs, t, :].astype(F32), bound[...])
            gates.append(jnp.where(t < count, g, 1.0))
            keys.append(jnp.where(t < count, 1.0 - g, 0.0))
        after = jnp.ones_like(gates[0])
        parts = [None] * 4
        for t in (3, 2, 1, 0):
            parts[t] = two_parts(keys[t] * after)
            after = after * gates[t]
        left = jnp.concatenate([p[0] for p in parts] + [p[1] for p in parts] + list(two_parts(after)), axis=0)
        values = jnp.concatenate([old_value[seqs, t, :].astype(F32) for t in range(4)] * 2, axis=0)
        values = jnp.concatenate([values, jnp.zeros((16, 256), F32)], axis=0)
        for h in range(2):
            lanes = slice(128 * h, 128 * h + 128)
            right = []
            for j in range(8):
                own_rows = row80 % 8 == j
                right.append(jnp.where(own_rows, values[:, lanes], 0.0))
                right.append(jnp.where(own_rows & (row80 >= 64), 1.0, 0.0))
            both = lax.dot_general(
                left[:, lanes].astype(BF16), jnp.concatenate(right, axis=1).astype(BF16),
                (((0,), (0,)), ((), ())), preferred_element_type=F32,
            )
            for j in range(8):
                added = both[:, 256 * j : 256 * j + 128]
                decay = both[:, 256 * j + 128 : 256 * j + 256]
                after_j = taken[8 * i + j, h] * decay + added
                taken[8 * i + j, h] = after_j
                packed[8 * i + j, h] = after_j.astype(BF16)

    step = lax.broadcasted_iota(jnp.int32, (64, 128), 0) % 4
    row16 = lax.broadcasted_iota(jnp.int32, (16, 128), 0)

    def give(b):
        for u in range(4):
            away[b, u] = sums[u, 256 + 64 * b : 320 + 64 * b].astype(BF16)

    def recur(n, b):
        rows = slice(64 * b, 64 * b + 64)
        h = 1 - head if n else head
        parts = (given[b, u] if n else sums[u, rows].astype(BF16) for u in range(4))
        q, p, v, gate = (part.astype(F32) for part in parts)
        q = q * 128 ** -0.5
        g = gate_of(p, bound[:, columns(h)])
        k = 1.0 - g
        decay = g
        total = jnp.sum(q * k, axis=-1, keepdims=True) * v
        reach = jnp.where(step == 0, g, 0.0)
        for lag in (1, 2, 3):
            score = jnp.sum(q * decay * pltpu.roll(k, lag, 0), axis=-1, keepdims=True)
            total = total + jnp.where(step >= lag, score * pltpu.roll(v, lag, 0), 0.0)
            decay = decay * pltpu.roll(g, lag, 0)
            reach = jnp.where(step == lag, decay, reach)
        queries[...] = (q * reach).astype(BF16)
        rest[...] = total
        for four in range(4):
            part = slice(16 * four, 16 * four + 16)
            lhs = queries[part]
            found = rest[part]
            for j in range(4):
                product = jnp.dot(lhs, packed[16 * b + 4 * four + j, h], preferred_element_type=F32)
                found = found + jnp.where(row16 // 4 == j, product, 0.0)
            rest[part] = found
        total = rest[...]
        scaled = total * lax.rsqrt(jnp.mean(total * total, axis=-1, keepdims=True) + EPSILON)
        heads[2 * me + h, rows] = (
            scaled * head_gain[:, columns(h)] * (gate * jax.nn.sigmoid(gate))
        ).astype(BF16)

    run = {
        "start": start, "wait": wait, "norm": norm, "norm2": norm2, "take": take, "product": product,
        "away": give, "recur": recur,
    }
    for name, *details in plan()[0]:
        run[name](*details)

    for sent, sem in (
        (gathered.at[:, pl.ds(0, 15)], send_sem),
        (out_weights.at[pl.ds(0, 15)], out_send),
        (heads.at[pl.ds(0, 14)], head_send),
        (raw_more, token_send),
        (given, given_send),
    ):
        pltpu.make_async_copy(sent, sent, sem).wait()


def layer_of(*arrays):
    outside = pl.BlockSpec(memory_space=pltpu.HBM)
    return pl.pallas_call(
        layer_kernel,
        in_specs=[outside] * 13,
        out_specs=[pl.BlockSpec(memory_space=pltpu.VMEM)] * 3,
        out_shape=[
            pltpu.VMEM((64, 2, 128, 128), F32),
            pltpu.VMEM((16, 256, 128), BF16),
            pltpu.VMEM((16, 128, 512), BF16),
        ],
        scratch_shapes=[
            pltpu.VMEM((256, 4096), BF16),
            pltpu.VMEM((8, 32, 4096), BF16),
            pltpu.VMEM((16, 512, 256), BF16),
            pltpu.VMEM((4, 16, 256, 128), BF16),
            pltpu.VMEM((4, 512, 128), F32),
            pltpu.VMEM((4, 4, 64, 128), BF16),
            pltpu.VMEM((4, 4, 64, 128), BF16),
            pltpu.VMEM((64, 2, 128, 128), BF16),
            pltpu.VMEM((64, 128), BF16),
            pltpu.VMEM((64, 128), F32),
            pltpu.VMEM((1, 4096), F32),
            pltpu.VMEM((1, 256), F32),
            pltpu.VMEM((1, 256), F32),
            pltpu.VMEM((64, 4, 256), BF16),
            pltpu.VMEM((64, 4, 256), BF16),
            pltpu.SMEM((64,), jnp.int32),
            pltpu.SemaphoreType.DMA,
            pltpu.SemaphoreType.DMA,
            pltpu.SemaphoreType.DMA,
            pltpu.SemaphoreType.DMA,
            pltpu.SemaphoreType.DMA,
            pltpu.SemaphoreType.DMA((64,)),
            pltpu.SemaphoreType.DMA((64,)),
            pltpu.SemaphoreType.DMA((16,)),
            pltpu.SemaphoreType.DMA((64,)),
            pltpu.SemaphoreType.DMA((4,)),
            pltpu.SemaphoreType.DMA((12,)),
            pltpu.SemaphoreType.DMA((8,)),
        ],
        compiler_params=pltpu.CompilerParams(
            collective_id=0, has_side_effects=True, vmem_limit_bytes=36 * 2**20
        ),
        name="layer",
    )(*(pltpu.with_memory_space_constraint(a, pltpu.HBM) for a in arrays))


def finish_kernel(taken_in, heads, out_weights, mixed, taken, block, sems):
    copy = pltpu.make_async_copy(taken_in, taken, sems.at[0])
    copy.start()
    for half in range(2):
        rows = slice(128 * half, 128 * half + 128)
        total = jnp.zeros((128, 512), F32)
        for h in range(16):
            total = total + jnp.dot(heads[h, rows], out_weights[h], preferred_element_type=F32)
        block[rows] = total.astype(BF16)
    last = pltpu.make_async_copy(block, mixed, sems.at[1])
    last.start()
    copy.wait()
    last.wait()


def finish_of(taken, heads, out_weights):
    inside = pl.BlockSpec(memory_space=pltpu.VMEM)
    anywhere = pl.BlockSpec(memory_space=pl.ANY)
    return pl.pallas_call(
        finish_kernel,
        in_specs=[inside] * 3,
        out_specs=[anywhere] * 2,
        out_shape=[jax.ShapeDtypeStruct((256, 512), BF16), jax.ShapeDtypeStruct(taken.shape, F32)],
        scratch_shapes=[pltpu.VMEM((256, 512), BF16), pltpu.SemaphoreType.DMA((2,))],
        compiler_params=pltpu.CompilerParams(vmem_limit_bytes=8 * 2**20),
        name="finish",
    )(*(pltpu.with_memory_space_constraint(a, pltpu.VMEM) for a in (taken, heads, out_weights)))


def on_device(
    tokens, norm_gain, w_query, w_forget, w_value, w_gate, lower_bound, head_gain, w_out,
    state, prev_forget, prev_value, accepted,
):
    return finish_of(*layer_of(
        accepted, tokens, norm_gain.reshape(1, 4096), w_query, w_forget, w_value, w_gate,
        lower_bound.reshape(1, 256), head_gain.reshape(1, 256), w_out, state, prev_forget, prev_value,
    ))


def solution(mesh):
    finer = Mesh(mesh.devices.reshape(4, 4, 4, 2), ("z", "y", "x", "c"))
    kv, tp = ("z", "y"), ("x", "c")
    placed = (
        P(kv, None), P(), P(kv, tp), P(kv, tp), P(kv, tp), P(kv, tp), P(tp), P(tp), P(kv, tp),
        P(kv, tp, None, None), P(kv, None, tp), P(kv, None, tp), P(kv),
    )
    return jax.shard_map(
        on_device, mesh=finer, in_specs=placed,
        out_specs=(P(kv, tp), P(kv, tp, None, None)), check_vma=False,
    )
```

time: 215 us -> 71.2 us (0.33)
  matrix products: 74.3 us -> 0 us
  waiting for transfers between devices: 71 us -> 0 us
  Pallas kernels: 0 us -> 70.4 us
  other arithmetic: 27.6 us -> 0 us
  between operations: 14.4 us -> 0.64 us
  blocking collectives: 13.3 us -> 0 us
  local copies, waits for them, and re-layouts: 9.11 us -> 0 us
  starting transfers between devices: 5.19 us -> 0 us
    dot_general x9 -> x0, matrix products: 74.3 us -> none  [the longest x4 59.7 us: recur_one(): outputs.append(jnp.einsum('hd,hde->he', queries[position], carried))]
    pallas_call x0 -> x2, Pallas kernels: none -> 70.4 us  [the longest x1 66.9 us: layer_of(): pl.pallas_call(layer_kernel, in_specs=[outside] * 13, out_specs=[pl.Block...]
    all_gather x2 -> x0, waiting for transfers between devices: 56 us -> none  [the longest x1 56 us: in_one_piece(): lax.all_gather(both, axis, axis=dim, tiled=True)]
    add x2 -> x0, other arithmetic: 19.9 us -> none  [the longest x1 19.9 us: recur_one(): decay_rate[:, :, None] * carried]
    all_to_all x1 -> x0, waiting for transfers between devices: 15 us -> none  [sent_to_all(): lax.all_to_all(jnp.broadcast_to(array[None], (size, *array.shape)), axis,...]
    all_gather x1 -> x0, blocking collectives: 13.3 us -> none  [gathered_by_axis(): nearer = lax.all_gather(array, axes[-1], axis=dim, tiled=True)]
    all_to_all x1 -> x0, starting transfers between devices: 5.11 us -> none  [sent_to_all(): lax.all_to_all(jnp.broadcast_to(array[None], (size, *array.shape)), axis,...]
    mul x8 -> x0, local copies, waits for them, and re-layouts: 4.48 us -> none  [the longest x5 2.56 us: recur_one(): forget[position][:, :, None] * carried]
  transfers between devices with their start and end apart: 3 -> 0, of which waited for: 2 -> 0; matrix products, arithmetic and copies ran while one was open for 49% -> 0% of each run, Pallas kernels for 0% -> 0%
where the time goes in v2:
time: 71.2 us; the launch traced here: 71.1 us
  Pallas kernels  70.4 us (99%)
    pallas_call x1, Pallas kernels, layer_of(): pl.pallas_call(layer_kernel, in_specs=[outside] * 13, out_specs=[pl.Block...  66.9 us
    pallas_call x1, Pallas kernels, finish_of(): pl.pallas_call(finish_kernel, in_specs=[inside] * 3, out_specs=[anywhere]...  3.49 us

profile of v2, /device:TPU:1, one launch (start us, length us, event | category | flops | bytes accessed | tf_op | source)
XLA Modules:
  0.0 71.1 jit_solution(3400896207019499216)
XLA Ops:
  0.6 66.9 %layer.1 = (f32[64,2,128,128]{3,2,1,0:T(8,128)S(1)}, bf16[16,256,128]{2,1,0:T(8,128)(2,1)S(1)}, bf16[16,128,512]{2,1,0:T(8,128)(2,1)S(1)}) custom-call(s32[64]{0:T(128)} %accepted_in.1, bf16[256,4096]{1,0:T(8,128)(2,1)} %tokens.1, f32[1,4096]{1,0:T(1,128)} %bitcast.3, bf16[256,256]{1,0:T(8,128)(2,1)} %w0.1, bf16[256,256]{1,0:T(8,128)(2,1)} %w1.1, ...), custom_call_target="tpu_custom_call" | custom-call | tf_op jit(solution)/shard_map/layer/pallas_call | solution.py:401
  67.6 3.5 %finish.1 = (bf16[256,512]{1,0:T(8,128)(2,1)}, f32[64,2,128,128]{3,2,1,0:T(8,128)}) custom-call(f32[64,2,128,128]{3,2,1,0:T(8,128)S(1)} %get-tuple-element.5.taken_in, bf16[16,256,128]{2,1,0:T(8,128)(2,1)S(1)} %get-tuple-element.6.heads, bf16[16,128,512]{2,1,0:T(8,128)(2,1)S(1)} %get-tuple-element.7.out_weights), custom_call_target="tpu_custom_call" | custom-call | tf_op jit(solution)/shard_map/finish/pallas_call | solution.py:465

commit v3 on v2

--- a/solution.py
+++ b/solution.py
@@ -13,7 +13,7 @@
 MESH = pl.DeviceIdType.MESH
 F32, BF16 = jnp.float32, jnp.bfloat16
 
-SIGN = ("z+", "z-", "z+", "z-")
+STAGES = ((0, 2), (1, 3))
 
 
 def shifted(dz, link):
@@ -22,36 +22,15 @@
 
 def sends(item):
     kind = item[0]
-    if kind == "w":
+    if kind in "wo":
         _, u, s, dz, dy = item
-        way = SIGN[u]
-        other = "z-" if way == "z+" else "z+"
-        links = []
-        if u < 2:
-            if dy == 0:
-                if dz == 0:
-                    links = [way, other]
-                elif dz == (3 if way == "z+" else 1):
-                    links = [way]
-                links = links + ["yi"]
-        else:
-            if dz == 0:
-                links = (["yi"] if dy == 0 else []) + [way, other]
-            elif dz == (3 if way == "z+" else 1):
-                links = [way]
-        return [(k, ("w", u, s, shifted(dz, k), 1 if k == "yi" else dy)) for k in links]
-    if kind == "o":
-        _, u, dz, dy = item
-        way = SIGN[u]
-        other = "z-" if way == "z+" else "z+"
-        along_y = {0: ["yi", "yo"], 1: ["yo"]}.get(dy, [])
+        way, other = ("z+", "z-") if (u // 2 + s) % 2 == 0 else ("z-", "z+")
         along_z = [way, other] if dz == 0 else [way] if dz == (3 if way == "z+" else 1) else []
         if u < 2:
-            links = along_y + along_z if dz == 0 else along_z
+            links = along_z + ["yi"] if dy == 0 else []
         else:
-            links = along_z + along_y if dy == 0 else along_y
-        turned = {("yi", 0): 1, ("yo", 0): 3, ("yo", 1): 2}
-        return [(k, ("o", u, shifted(dz, k), turned.get((k, dy), dy))) for k in links]
+            links = (["yi"] if dy == dz == 0 else []) + along_z
+        return [(k, (kind, u, s, shifted(dz, k), 1 if k == "yi" else dy)) for k in links]
     if kind in "th":
         at, b = item[-2], item[-1]
         first, over = item[:-2], {"t": "u", "h": "g"}[kind]
@@ -66,25 +45,31 @@
     return []
 
 
-SIZE = {"w": 64, "o": 32, "t": 128, "u": 128, "h": 16, "g": 16, "q": 64}
-OUT_AT = 20
-TIMES = {"norm": 2.2, "norm2": 2.2, "take": 1.4, "product": 0.17, "away": 0.15, "recur": 0.4}
+SIZE = {"w": 64, "o": 32, "t": 128, "u": 128, "h": 16, "g": 16}
+SECOND_AT, OUT_AT = 1, 60
+FIRST_SENDS = (
+    ("t", 0), ("t", 1), ("w", 0), ("w", 2), ("w", 1), ("w", 3), ("o", 0), ("o", 1), ("o", 2), ("o", 3),
+)
+TIMES = {"norm": 0.6, "norm2": 0.15, "take": 0.7, "product": 0.04, "away": 0.05, "recur": 0.4}
 
 
 @functools.cache
 def plan():
-    free, events, steps = {}, [], []
-    now, count, arrived_w, out_started = 0.0, 0, 0, False
-    done, ready = set(), []
-    work = [("norm",)] + [("take", i) for i in range(8)]
-    products = [(u, 0, 0, 0) for u in range(4)]
-    stage = {"tokens": 0, "products": 0, "recur": 0}
+    free, events, steps, marks = {}, [], [], {}
+    now, count, got = 0.0, 0, 0
+    soon = [("norm", i) for i in range(4)]
+    later = [("take", i, h) for i in range(8) for h in range(2)]
+    products = {(stage, half): [] for stage in range(2) for half in range(2)}
+    left = dict.fromkeys(products, 32)
+    tokens = 16
+    held = [("o", u, 0, 0, 0) for u in range(4)]
+    returned = set()
 
     def send(item, link, there):
         nonlocal count
         begin = max(now, free.get(link, 0.0))
-        rate = 0.0017 if link == "c" else 0.0215
-        free[link] = begin + SIZE[item[0]] * rate
+        size = (128 if item[1] == 0 else 32) if item[0] == "q" else SIZE[item[0]]
+        free[link] = begin + size * (0.0017 if link == "c" else 0.0225)
         count += 1
         heapq.heappush(events, (free[link] + (1.0 if link == "c" else 2.2), count, there))
         steps.append(("start", item, link, there))
@@ -93,57 +78,100 @@
         for link, there in sends(item):
             send(item, link, there)
 
-    own = [("w", u, 0, 0, 0) for u in range(4)]
-    for u in (0, 2, 1, 3):
-        send(("w", u, 1, None, None), "yo", ("w", u, 1, 0, 0))
-        if u in (0, 1):
-            send(("t", 0, u), "yo", ("t", 0, u))
-    for item in own:
-        go_on(item)
+    def swap(kind, u):
+        send((kind, u, 1, None, None), "yo", (kind, u, 1, 0, 0))
+
+    def add(u, *rest):
+        for half in range(2):
+            products[u % 2, half].append((half, u, *rest))
+
+    def begin(which):
+        for u in STAGES[which]:
+            add(u, 0, 0, 0)
+            go_on(("w", u, 0, 0, 0))
+
+    def recur(n, b):
+        soon.append(("recur", n, b))
+
+    for step in FIRST_SENDS:
+        if step[0] == "t":
+            send(("t", 0, step[1]), "yo", ("t", 0, step[1]))
+        else:
+            swap(*step)
+    begin(0)
 
     def task():
-        if work and work[0][0] == "norm":
-            return work.pop(0)
-        if stage["tokens"] == 16:
-            stage["tokens"] = 0
-            stage["ready"] = 1
-            return ("norm2",)
-        if "ready" in stage and products:
-            stage["products"] += 1
-            if stage["products"] == 64:
-                work.extend([("away", b) for b in range(4)] + [("recur", 0, b) for b in range(4)])
-            return ("product", *products.pop(0))
-        return work.pop(0) if work else None
+        for key in ((0, 0), (0, 1), (1, 0), (1, 1)):
+            if products[key] and not (soon and soon[0][0] == "norm") and not (key[1] and tokens):
+                left[key] -= 1
+                job = ("product", *products[key].pop(0))
+                if left[key] == 0 and key[1]:
+                    soon[:0] = [("away", key[0], b) for b in range(4)]
+                if key[0] and left[1, 0] == left[1, 1] == 0:
+                    soon.extend(later)
+                    later.clear()
+                    for b in range(4):
+                        recur(0, b)
+                return job
+            if soon and soon[0][0] in ("norm2", "away"):
+                break
+        if soon:
+            return soon.pop(0)
+        return later.pop(0) if later else None
 
     while True:
         if events and events[0][0] <= now:
             _, _, item = heapq.heappop(events)
             steps.append(("wait", item))
+            now += 0.02
+            if item[0] == "o" and item[2:] == (1, 0, 0) and held is not None:
+                held.append(item)
+                continue
             go_on(item)
             if item[0] == "w":
-                products.append(item[1:])
-                arrived_w += 1
-                if arrived_w == OUT_AT:
-                    for u in range(4):
-                        go_on(("o", u, 0, 0))
+                add(*item[1:])
+                got += 1
+                if got == SECOND_AT:
+                    begin(1)
+                if got == OUT_AT:
+                    for other in held:
+                        go_on(other)
+                    held = None
+                if got == 60:
+                    marks["weights"] = now
             elif item[0] in "tu":
-                stage["tokens"] += 1
+                tokens -= 1
+                steps.append(("norm2", item))
+                now += TIMES["norm2"]
+                if tokens == 0:
+                    marks["tokens"] = now
             elif item[0] == "q":
-                work.append(("recur", 1, item[1]))
-            now += 0.02
+                returned.add(item[1:])
+                marks["q", *item[1:]] = now
+                for b in range(4):
+                    if (0, 0) in returned and (1, b) in returned:
+                        returned.remove((1, b))
+                        recur(1, b)
+            elif item[0] == "o":
+                marks["o"] = now
             continue
         job = task()
         if job is not None:
             steps.append(job)
             now += TIMES[job[0]]
             if job[0] == "away":
-                send(("q", job[1]), "yo", ("q", job[1]))
+                if job[1] == 1:
+                    send(("q", 1, job[2]), "yo", ("q", 1, job[2]))
+                elif job[2] == 3:
+                    send(("q", 0, 0), "yo", ("q", 0, 0))
             elif job[0] == "recur":
                 go_on(("h", job[1], 0, job[2]))
+                marks["recur"] = now
         elif events:
             now = events[0][0]
         else:
-            return tuple(steps), now
+            marks["end"] = now
+            return tuple(steps), now, marks
 
 
 def gate_of(pre_act, bound):
@@ -213,14 +241,11 @@
 
     def place(item, core):
         kind = item[0]
-        if kind == "w":
+        if kind in "wo":
             _, u, s, dz, dy = item
             row = y if dy == 0 else inner
-            return gathered.at[u, (z + dz) % 4 * 4 + (3 - row if s else row)]
-        if kind == "o":
-            _, u, dz, dy = item
-            row = (y, inner, (y + 2) % 4, outer)[dy]
-            return out_weights.at[(z + dz) % 4 * 4 + row, pl.ds(32 * u, 32)]
+            k = (z + dz) % 4 * 4 + (3 - row if s else row)
+            return gathered.at[u, k] if kind == "w" else out_weights.at[k, pl.ds(32 * u, 32)]
         if kind in "tu":
             _, at, part = item
             return raw_more.at[chip(at) * 2 + core, pl.ds(16 * part, 16)]
@@ -228,22 +253,19 @@
             _, n, at, b = item
             which = (chip(at) * 2 + core) * 2 + (1 - head if n else head)
             return heads.at[which, pl.ds(64 * b, 64)]
-        return given.at[item[1]]
+        return given.at[0] if item[1] == 0 else given.at[1, item[2]]
 
     def arrival(item):
         kind = item[0]
-        if kind == "w":
+        if kind in "wo":
             _, u, s, dz, dy = item
-            return w_recv.at[u * 16 + s * 8 + dz * 2 + dy]
-        if kind == "o":
-            _, u, dz, dy = item
-            return o_recv.at[u * 16 + dz * 4 + dy]
+            return (w_recv if kind == "w" else o_recv).at[u * 16 + s * 8 + dz * 2 + dy]
         if kind in "tu":
             return t_recv.at[(8 if kind == "u" else 0) + item[1] * 2 + item[2]]
         if kind in "hg":
             _, n, at, b = item
             return h_recv.at[(32 if kind == "g" else 0) + n * 16 + at * 4 + b]
-        return q_recv.at[item[1]]
+        return q_recv.at[item[1] * 4 + item[2]]
 
     leaving = {"w": send_sem, "o": out_send, "t": token_send, "h": head_send, "q": given_send}
 
@@ -253,13 +275,15 @@
             source, to = weights[item[1]].at[:, columns(1 - head)], gathered.at[item[1], mine]
         elif kind == "w" and item[2:] == (0, 0, 0):
             source, to = weights[item[1]].at[:, columns(head)], gathered.at[item[1], mine]
-        elif kind == "o" and item[2:] == (0, 0):
-            source, to = w_out.at[pl.ds(32 * item[1], 32)], place(item, c)
+        elif kind == "o" and (item[3] is None or item[2:] == (0, 0, 0)):
+            rows = pl.ds(32 * item[1], 32)
+            source, to = w_out.at[rows], out_weights.at[mine, rows]
         elif kind == "t" and link == "yo":
             rows = pl.ds(pl.multiple_of(32 * me + 16 * item[2], 16), 16)
             source, to = tokens.at[rows], place(item, c)
         elif kind == "q":
-            source, to = away.at[item[1]], given.at[item[1]]
+            to = place(item, c)
+            source = away.at[0] if item[1] == 0 else away.at[1, item[2]]
         else:
             source = to = place(item, c)
         pltpu.make_async_remote_copy(
@@ -271,47 +295,56 @@
         ref = place(item, 1 - c if item[0] in "ug" else c)
         pltpu.make_async_copy(ref, ref, arrival(item)).wait()
 
-    def normalize(take_rows, first):
-        @pl.loop(0, 16)
+    def normalize(rows_in, first):
+        floated = rows_in.astype(F32)
+        scale = lax.rsqrt(jnp.mean(floated * floated, axis=-1, keepdims=True) + EPSILON)
+        scaled = (floated * scale * gain[...]).astype(BF16)
+        rows = pl.ds(pl.multiple_of(first, 16), 16)
+        for k in range(16):
+            normed[k, rows, :] = scaled[:, 256 * k : 256 * k + 256]
+
+    def norm(quarter):
+        if quarter == 0:
+            for copy in token_copies:
+                copy.wait()
+
+        @pl.loop(4 * quarter, 4 * quarter + 4)
         def _(i):
-            floated = take_rows(i).astype(F32)
-            scale = lax.rsqrt(jnp.mean(floated * floated, axis=-1, keepdims=True) + EPSILON)
-            scaled = (floated * scale * gain[...]).astype(BF16)
-            rows = pl.ds(pl.multiple_of(first + 16 * i, 16), 16)
-            for k in range(16):
-                normed[k, rows, :] = scaled[:, 256 * k : 256 * k + 256]
-
-    def norm():
-        for copy in token_copies:
-            copy.wait()
-        normalize(lambda i: raw[pl.ds(pl.multiple_of(16 * i, 16), 16), :], 0)
-        for copy in own_copies + small_copies:
-            copy.wait()
-
-    def norm2():
-        normalize(lambda i: raw_more[i // 2, pl.ds(pl.multiple_of(i % 2 * 16, 16), 16), :], 256)
+            normalize(raw[pl.ds(pl.multiple_of(16 * i, 16), 16), :], 16 * i)
+
+        if quarter == 3:
+            for copy in own_copies + small_copies:
+                copy.wait()
+
+    def norm2(item):
+        _, kind, part = item
+        piece = chip(kind) * 2 + (1 - c if item[0] == "u" else c)
+        normalize(raw_more[piece, 16 * part : 16 * part + 16, :], 256 + 32 * piece + 16 * part)
 
     begun = set()
 
-    def product(u, s, dz, dy):
+    def product(half, u, s, dz, dy):
         row = y if dy == 0 else inner
         k = (z + dz) % 4 * 4 + (3 - row if s else row)
-        found = jnp.dot(normed[k], gathered[u, k], preferred_element_type=F32)
-        sums[u] = sums[u] + found if u in begun else found
-        begun.add(u)
-
-    row8 = lax.broadcasted_iota(jnp.int32, (8, 256), 0)
+        rows = slice(256 * half, 256 * half + 256)
+        found = jnp.dot(normed[k, rows], gathered[u, k], preferred_element_type=F32)
+        sums[u, rows] = sums[u, rows] + found if (half, u) in begun else found
+        begun.add((half, u))
+
+    row8 = lax.broadcasted_iota(jnp.int32, (8, 128), 0)
     row80 = lax.broadcasted_iota(jnp.int32, (80, 128), 0)
 
-    def take(i):
-        state_copy(i).wait()
-        seqs = pl.ds(pl.multiple_of(8 * i, 8), 8)
-        count = jnp.zeros((8, 256), jnp.int32)
+    def take(i, h):
+        if h == 0:
+            state_copy(i).wait()
+        lanes = slice(128 * h, 128 * h + 128)
+        seqs = slice(8 * i, 8 * i + 8)
+        count = jnp.zeros((8, 128), jnp.int32)
         for j in range(8):
             count = jnp.where(row8 == j, accepted[8 * i + j], count)
         gates, keys = [], []
         for t in range(4):
-            g = gate_of(old_forget[seqs, t, :].astype(F32), bound[...])
+            g = gate_of(old_forget[seqs, t, lanes].astype(F32), bound[:, lanes])
             gates.append(jnp.where(t < count, g, 1.0))
             keys.append(jnp.where(t < count, 1.0 - g, 0.0))
         after = jnp.ones_like(gates[0])
@@ -320,37 +353,35 @@
             parts[t] = two_parts(keys[t] * after)
             after = after * gates[t]
         left = jnp.concatenate([p[0] for p in parts] + [p[1] for p in parts] + list(two_parts(after)), axis=0)
-        values = jnp.concatenate([old_value[seqs, t, :].astype(F32) for t in range(4)] * 2, axis=0)
-        values = jnp.concatenate([values, jnp.zeros((16, 256), F32)], axis=0)
-        for h in range(2):
-            lanes = slice(128 * h, 128 * h + 128)
-            right = []
-            for j in range(8):
-                own_rows = row80 % 8 == j
-                right.append(jnp.where(own_rows, values[:, lanes], 0.0))
-                right.append(jnp.where(own_rows & (row80 >= 64), 1.0, 0.0))
-            both = lax.dot_general(
-                left[:, lanes].astype(BF16), jnp.concatenate(right, axis=1).astype(BF16),
-                (((0,), (0,)), ((), ())), preferred_element_type=F32,
-            )
-            for j in range(8):
-                added = both[:, 256 * j : 256 * j + 128]
-                decay = both[:, 256 * j + 128 : 256 * j + 256]
-                after_j = taken[8 * i + j, h] * decay + added
-                taken[8 * i + j, h] = after_j
-                packed[8 * i + j, h] = after_j.astype(BF16)
+        values = [old_value[seqs, t, lanes].astype(F32) for t in range(4)] * 2
+        values = jnp.concatenate(values + [jnp.zeros((16, 128), F32)], axis=0)
+        right = []
+        for j in range(8):
+            own_rows = row80 % 8 == j
+            right.append(jnp.where(own_rows, values, 0.0))
+            right.append(jnp.where(own_rows & (row80 >= 64), 1.0, 0.0))
+        both = lax.dot_general(
+            left.astype(BF16), jnp.concatenate(right, axis=1).astype(BF16),
+            (((0,), (0,)), ((), ())), preferred_element_type=F32,
+        )
+        for j in range(8):
+            added = both[:, 256 * j : 256 * j + 128]
+            decay = both[:, 256 * j + 128 : 256 * j + 256]
+            after_j = taken[8 * i + j, h] * decay + added
+            taken[8 * i + j, h] = after_j
+            packed[8 * i + j, h] = after_j.astype(BF16)
 
     step = lax.broadcasted_iota(jnp.int32, (64, 128), 0) % 4
     row16 = lax.broadcasted_iota(jnp.int32, (16, 128), 0)
 
-    def give(b):
-        for u in range(4):
-            away[b, u] = sums[u, 256 + 64 * b : 320 + 64 * b].astype(BF16)
+    def give(stage, b):
+        for i, u in enumerate(STAGES[stage]):
+            away[stage, b, i] = sums[u, 256 + 64 * b : 320 + 64 * b].astype(BF16)
 
     def recur(n, b):
         rows = slice(64 * b, 64 * b + 64)
         h = 1 - head if n else head
-        parts = (given[b, u] if n else sums[u, rows].astype(BF16) for u in range(4))
+        parts = (given[u % 2, b, u // 2] if n else sums[u, rows].astype(BF16) for u in range(4))
         q, p, v, gate = (part.astype(F32) for part in parts)
         q = q * 128 ** -0.5
         g = gate_of(p, bound[:, columns(h)])
@@ -413,8 +444,8 @@
             pltpu.VMEM((16, 512, 256), BF16),
             pltpu.VMEM((4, 16, 256, 128), BF16),
             pltpu.VMEM((4, 512, 128), F32),
-            pltpu.VMEM((4, 4, 64, 128), BF16),
-            pltpu.VMEM((4, 4, 64, 128), BF16),
+            pltpu.VMEM((2, 4, 2, 64, 128), BF16),
+            pltpu.VMEM((2, 4, 2, 64, 128), BF16),
             pltpu.VMEM((64, 2, 128, 128), BF16),
             pltpu.VMEM((64, 128), BF16),
             pltpu.VMEM((64, 128), F32),
@@ -433,7 +464,7 @@
             pltpu.SemaphoreType.DMA((64,)),
             pltpu.SemaphoreType.DMA((16,)),
             pltpu.SemaphoreType.DMA((64,)),
-            pltpu.SemaphoreType.DMA((4,)),
+            pltpu.SemaphoreType.DMA((8,)),
             pltpu.SemaphoreType.DMA((12,)),
             pltpu.SemaphoreType.DMA((8,)),
         ],

time: 71.2 us -> 60.7 us (0.85)
  Pallas kernels: 70.4 us -> 59.9 us
    pallas_call x1, Pallas kernels: 66.9 us -> 56.4 us  [layer_of(): pl.pallas_call(layer_kernel, in_specs=[outside] * 13, out_specs=[pl.Block...]
where the time goes in v3:
time: 60.7 us; the launch traced here: 60.6 us
  Pallas kernels  59.9 us (99%)
  between operations  0.64 us (1%)
    pallas_call x1, Pallas kernels, layer_of(): pl.pallas_call(layer_kernel, in_specs=[outside] * 13, out_specs=[pl.Block...  56.4 us
    pallas_call x1, Pallas kernels, finish_of(): pl.pallas_call(finish_kernel, in_specs=[inside] * 3, out_specs=[anywhere]...  3.49 us

profile of v3, /device:TPU:1, one launch (start us, length us, event | category | flops | bytes accessed | tf_op | source)
XLA Modules:
  0.0 60.6 jit_solution(4919859436892138637)
XLA Ops:
  0.6 56.4 %layer.1 = (f32[64,2,128,128]{3,2,1,0:T(8,128)S(1)}, bf16[16,256,128]{2,1,0:T(8,128)(2,1)S(1)}, bf16[16,128,512]{2,1,0:T(8,128)(2,1)S(1)}) custom-call(s32[64]{0:T(128)} %accepted_in.1, bf16[256,4096]{1,0:T(8,128)(2,1)} %tokens.1, f32[1,4096]{1,0:T(1,128)} %bitcast.3, bf16[256,256]{1,0:T(8,128)(2,1)} %w0.1, bf16[256,256]{1,0:T(8,128)(2,1)} %w1.1, ...), custom_call_target="tpu_custom_call" | custom-call | tf_op jit(solution)/shard_map/layer/pallas_call | solution.py:432
  57.1 3.5 %finish.1 = (bf16[256,512]{1,0:T(8,128)(2,1)}, f32[64,2,128,128]{3,2,1,0:T(8,128)}) custom-call(f32[64,2,128,128]{3,2,1,0:T(8,128)S(1)} %get-tuple-element.5.taken_in, bf16[16,256,128]{2,1,0:T(8,128)(2,1)S(1)} %get-tuple-element.6.heads, bf16[16,128,512]{2,1,0:T(8,128)(2,1)S(1)} %get-tuple-element.7.out_weights), custom_call_target="tpu_custom_call" | custom-call | tf_op jit(solution)/shard_map/finish/pallas_call | solution.py:496

commit v4 on v3

--- a/solution.py
+++ b/solution.py
@@ -13,7 +13,10 @@
 MESH = pl.DeviceIdType.MESH
 F32, BF16 = jnp.float32, jnp.bfloat16
 
-STAGES = ((0, 2), (1, 3))
+LAST = 3
+DIRECT = (("h", 1),)
+Z_FIRST, UP = (False, False, True, True, False, False, True, True), (False, True, True, False, True, True, False, False)
+OUT_Z_FIRST, OUT_UP, OUT_BY_INNER = (False, False, True, True), (True, False, True, False), (False, False, True, False)
 
 
 def shifted(dz, link):
@@ -22,11 +25,24 @@
 
 def sends(item):
     kind = item[0]
-    if kind in "wo":
+    if kind == "o":
+        _, u, dz, r = item
+        way, other = ("z+", "z-") if OUT_UP[u] else ("z-", "z+")
+        along_z = [way, other] if dz == 0 else [way] if dz == (3 if way == "z+" else 1) else []
+        along_y = ["yo", "yi"] if r == 0 else []
+        if r == (1 if OUT_BY_INNER[u] else 3):
+            along_y = ["yo" if OUT_BY_INNER[u] else "yi"]
+        if OUT_Z_FIRST[u]:
+            links = along_z + along_y if r == 0 else along_y
+        else:
+            links = along_y + along_z if dz == 0 else along_z
+        turned = {("yi", 0): 1, ("yo", 0): 3, ("yo", 1): 2, ("yi", 3): 2}
+        return [(k, (kind, u, shifted(dz, k), turned.get((k, r), r))) for k in links]
+    if kind == "w":
         _, u, s, dz, dy = item
-        way, other = ("z+", "z-") if (u // 2 + s) % 2 == 0 else ("z-", "z+")
+        way, other = ("z+", "z-") if UP[2 * u + s] else ("z-", "z+")
         along_z = [way, other] if dz == 0 else [way] if dz == (3 if way == "z+" else 1) else []
-        if u < 2:
+        if Z_FIRST[2 * u + s]:
             links = along_z + ["yi"] if dy == 0 else []
         else:
             links = (["yi"] if dy == dz == 0 else []) + along_z
@@ -38,19 +54,20 @@
         if at == 0:
             go = [("x+", (*first, 1, b)), ("x-", (*first, 2, b))] + go
         elif at == 1 and b % 2 == 0:
-            go = [("x+", (*first, 3, b))] + go
+            go = [("x+", (*first, 3, b))] + ([("X+", (over, *first[1:], 3, b))] if first in DIRECT else []) + go
         elif at == 2 and b % 2 == 1:
-            go = [("x-", (*first, 3, b))] + go
+            go = [("x-", (*first, 3, b))] + ([("X-", (over, *first[1:], 3, b))] if first in DIRECT else []) + go
+        elif at == 3 and first in DIRECT:
+            go = []
         return go
     return []
 
 
 SIZE = {"w": 64, "o": 32, "t": 128, "u": 128, "h": 16, "g": 16}
-SECOND_AT, OUT_AT = 1, 60
-FIRST_SENDS = (
-    ("t", 0), ("t", 1), ("w", 0), ("w", 2), ("w", 1), ("w", 3), ("o", 0), ("o", 1), ("o", 2), ("o", 3),
-)
-TIMES = {"norm": 0.6, "norm2": 0.15, "take": 0.7, "product": 0.04, "away": 0.05, "recur": 0.4}
+SLACK = {"w": 0.6, "u": 1.0, "q": 0.5}
+BEGIN_AT, EARLY_AT, OUT_AT = (0, 0, 0, 16), 16, (54, 54)
+FIRST_SENDS = (("w", 1), ("t", 1), ("t", 0), ("w", 2), ("w", 0), ("w", 3))
+TIMES = {"norm": 0.6, "norm2": 0.15, "take": 0.4, "product": 0.1, "away": 0.05, "recur": 0.4}
 
 
 @functools.cache
@@ -59,36 +76,44 @@
     now, count, got = 0.0, 0, 0
     soon = [("norm", i) for i in range(4)]
     later = [("take", i, h) for i in range(8) for h in range(2)]
-    products = {(stage, half): [] for stage in range(2) for half in range(2)}
-    left = dict.fromkeys(products, 32)
+    products = [([], []) for _ in range(4)]
+    left = [[16, 16] for _ in range(4)]
     tokens = 16
-    held = [("o", u, 0, 0, 0) for u in range(4)]
-    returned = set()
+    held, shut = [], {"z+", "z-", "yi"}
+    returned, ends = set(), []
 
     def send(item, link, there):
         nonlocal count
-        begin = max(now, free.get(link, 0.0))
-        size = (128 if item[1] == 0 else 32) if item[0] == "q" else SIZE[item[0]]
-        free[link] = begin + size * (0.0017 if link == "c" else 0.0225)
+        lane = link.lower()
+        begin = max(now, free.get(lane, 0.0))
+        size = (16 if item[1] == LAST else 64) if item[0] == "q" else SIZE[item[0]]
+        free[lane] = begin + size * (0.0017 if link == "c" else 0.0225)
         count += 1
-        heapq.heappush(events, (free[link] + (1.0 if link == "c" else 2.2), count, there))
+        heapq.heappush(events, (free[lane] + (1.0 if link == "c" else 2.6), count, there))
         steps.append(("start", item, link, there))
 
     def go_on(item):
         for link, there in sends(item):
-            send(item, link, there)
-
-    def swap(kind, u):
-        send((kind, u, 1, None, None), "yo", (kind, u, 1, 0, 0))
+            if item[0] == "o" and link in shut:
+                held.append((item, link, there))
+            else:
+                send(item, link, there)
 
     def add(u, *rest):
         for half in range(2):
-            products[u % 2, half].append((half, u, *rest))
-
-    def begin(which):
-        for u in STAGES[which]:
-            add(u, 0, 0, 0)
-            go_on(("w", u, 0, 0, 0))
+            products[u][half].append((u, *rest))
+
+    def begin():
+        for u in range(4):
+            if BEGIN_AT[u] == got:
+                add(u, 0, 0, 0)
+                go_on(("w", u, 0, 0, 0))
+
+    def release(*links):
+        shut.difference_update(links)
+        for step in [step for step in held if step[1] in links]:
+            held.remove(step)
+            send(*step)
 
     def recur(n, b):
         soon.append(("recur", n, b))
@@ -97,46 +122,57 @@
         if step[0] == "t":
             send(("t", 0, step[1]), "yo", ("t", 0, step[1]))
         else:
-            swap(*step)
-    begin(0)
+            send(("w", step[1], 1, None, None), "yo", ("w", step[1], 1, 0, 0))
+    begin()
 
     def task():
-        for key in ((0, 0), (0, 1), (1, 0), (1, 1)):
-            if products[key] and not (soon and soon[0][0] == "norm") and not (key[1] and tokens):
-                left[key] -= 1
-                job = ("product", *products[key].pop(0))
-                if left[key] == 0 and key[1]:
-                    soon[:0] = [("away", key[0], b) for b in range(4)]
-                if key[0] and left[1, 0] == left[1, 1] == 0:
-                    soon.extend(later)
-                    later.clear()
-                    for b in range(4):
-                        recur(0, b)
-                return job
-            if soon and soon[0][0] in ("norm2", "away"):
-                break
+        if soon and soon[0][0] in ("norm", "norm2", "away"):
+            return soon.pop(0)
+        for u in range(4):
+            for half in range(2):
+                if products[u][half] and not (half and tokens):
+                    unit = products[u][half].pop(0)
+                    if half == 0 and not tokens:
+                        products[u][1].remove(unit)
+                        half = 2
+                    for one in range(2):
+                        left[u][one] -= half in (one, 2)
+                    if half and left[u][1] == 0:
+                        soon[:0] = [("away", u, b) for b in range(4)]
+                    if left[LAST] == [0, 0] or sum(map(sum, left)) == 0:
+                        soon.extend(later)
+                        later.clear()
+                    if sum(map(sum, left)) == 0:
+                        for b in range(4):
+                            recur(0, b)
+                    return ("product", half, *unit)
         if soon:
             return soon.pop(0)
         return later.pop(0) if later else None
 
     while True:
         if events and events[0][0] <= now:
-            _, _, item = heapq.heappop(events)
+            _, count_of, item = heapq.heappop(events)
+            if count_of > 0 and not sends(item):
+                if item[0] in "ogh":
+                    ends.append(item)
+                else:
+                    heapq.heappush(events, (now + (0.0 if got > 50 else SLACK[item[0]]), -count_of, item))
+                continue
             steps.append(("wait", item))
             now += 0.02
-            if item[0] == "o" and item[2:] == (1, 0, 0) and held is not None:
-                held.append(item)
-                continue
             go_on(item)
             if item[0] == "w":
                 add(*item[1:])
                 got += 1
-                if got == SECOND_AT:
-                    begin(1)
-                if got == OUT_AT:
-                    for other in held:
-                        go_on(other)
-                    held = None
+                begin()
+                if got == EARLY_AT:
+                    for u in range(4):
+                        go_on(("o", u, 0, 0))
+                if got == OUT_AT[0]:
+                    release("z+", "z-")
+                if got == OUT_AT[1]:
+                    release("yi")
                 if got == 60:
                     marks["weights"] = now
             elif item[0] in "tu":
@@ -149,8 +185,8 @@
                 returned.add(item[1:])
                 marks["q", *item[1:]] = now
                 for b in range(4):
-                    if (0, 0) in returned and (1, b) in returned:
-                        returned.remove((1, b))
+                    if all((u, 0) in returned for u in range(4) if u != LAST) and (LAST, b) in returned:
+                        returned.remove((LAST, b))
                         recur(1, b)
             elif item[0] == "o":
                 marks["o"] = now
@@ -160,10 +196,10 @@
             steps.append(job)
             now += TIMES[job[0]]
             if job[0] == "away":
-                if job[1] == 1:
-                    send(("q", 1, job[2]), "yo", ("q", 1, job[2]))
+                if job[1] == LAST:
+                    send(("q", LAST, job[2]), "yo", ("q", LAST, job[2]))
                 elif job[2] == 3:
-                    send(("q", 0, 0), "yo", ("q", 0, 0))
+                    send(("q", job[1], 0), "yo", ("q", job[1], 0))
             elif job[0] == "recur":
                 go_on(("h", job[1], 0, job[2]))
                 marks["recur"] = now
@@ -171,6 +207,7 @@
             now = events[0][0]
         else:
             marks["end"] = now
+            steps.extend(("wait", item) for item in ends)
             return tuple(steps), now, marks
 
 
@@ -200,6 +237,7 @@
     target = {
         "z+": {"z": (z + 1) % 4}, "z-": {"z": (z + 3) % 4}, "yi": {"y": inner}, "yo": {"y": outer},
         "x+": {"x": (x + 1) % 4}, "x-": {"x": (x + 3) % 4}, "c": {"c": 1 - c},
+        "X+": {"x": (x + 1) % 4, "c": 1 - c}, "X-": {"x": (x + 3) % 4, "c": 1 - c},
     }
 
     barrier = pltpu.get_barrier_semaphore()
@@ -241,11 +279,14 @@
 
     def place(item, core):
         kind = item[0]
-        if kind in "wo":
+        if kind == "w":
             _, u, s, dz, dy = item
             row = y if dy == 0 else inner
-            k = (z + dz) % 4 * 4 + (3 - row if s else row)
-            return gathered.at[u, k] if kind == "w" else out_weights.at[k, pl.ds(32 * u, 32)]
+            return gathered.at[u, (z + dz) % 4 * 4 + (3 - row if s else row)]
+        if kind == "o":
+            _, u, dz, r = item
+            row = (y, inner, (y + 2) % 4, outer)[r]
+            return out_weights.at[(z + dz) % 4 * 4 + row, pl.ds(32 * u, 32)]
         if kind in "tu":
             _, at, part = item
             return raw_more.at[chip(at) * 2 + core, pl.ds(16 * part, 16)]
@@ -253,13 +294,16 @@
             _, n, at, b = item
             which = (chip(at) * 2 + core) * 2 + (1 - head if n else head)
             return heads.at[which, pl.ds(64 * b, 64)]
-        return given.at[0] if item[1] == 0 else given.at[1, item[2]]
+        return given.at[item[1], pl.ds(64 * item[2], 64)] if item[1] == LAST else given.at[item[1]]
 
     def arrival(item):
         kind = item[0]
-        if kind in "wo":
+        if kind == "w":
             _, u, s, dz, dy = item
-            return (w_recv if kind == "w" else o_recv).at[u * 16 + s * 8 + dz * 2 + dy]
+            return w_recv.at[u * 16 + s * 8 + dz * 2 + dy]
+        if kind == "o":
+            _, u, dz, r = item
+            return o_recv.at[u * 16 + dz * 4 + r]
         if kind in "tu":
             return t_recv.at[(8 if kind == "u" else 0) + item[1] * 2 + item[2]]
         if kind in "hg":
@@ -275,15 +319,14 @@
             source, to = weights[item[1]].at[:, columns(1 - head)], gathered.at[item[1], mine]
         elif kind == "w" and item[2:] == (0, 0, 0):
             source, to = weights[item[1]].at[:, columns(head)], gathered.at[item[1], mine]
-        elif kind == "o" and (item[3] is None or item[2:] == (0, 0, 0)):
-            rows = pl.ds(32 * item[1], 32)
-            source, to = w_out.at[rows], out_weights.at[mine, rows]
+        elif kind == "o" and item[2:] == (0, 0):
+            source, to = w_out.at[pl.ds(32 * item[1], 32)], place(item, c)
         elif kind == "t" and link == "yo":
             rows = pl.ds(pl.multiple_of(32 * me + 16 * item[2], 16), 16)
             source, to = tokens.at[rows], place(item, c)
         elif kind == "q":
             to = place(item, c)
-            source = away.at[0] if item[1] == 0 else away.at[1, item[2]]
+            source = away.at[item[1], pl.ds(64 * item[2], 64)] if item[1] == LAST else away.at[item[1]]
         else:
             source = to = place(item, c)
         pltpu.make_async_remote_copy(
@@ -324,12 +367,15 @@
     begun = set()
 
     def product(half, u, s, dz, dy):
+        if half == 2 and ((0, u) in begun) != ((1, u) in begun):
+            product(0, u, s, dz, dy)
+            return product(1, u, s, dz, dy)
         row = y if dy == 0 else inner
         k = (z + dz) % 4 * 4 + (3 - row if s else row)
-        rows = slice(256 * half, 256 * half + 256)
+        rows = slice(0, 512) if half == 2 else slice(256 * half, 256 * half + 256)
         found = jnp.dot(normed[k, rows], gathered[u, k], preferred_element_type=F32)
-        sums[u, rows] = sums[u, rows] + found if (half, u) in begun else found
-        begun.add((half, u))
+        sums[u, rows] = sums[u, rows] + found if (half % 2, u) in begun else found
+        begun.update((one, u) for one in range(2) if half in (one, 2))
 
     row8 = lax.broadcasted_iota(jnp.int32, (8, 128), 0)
     row80 = lax.broadcasted_iota(jnp.int32, (80, 128), 0)
@@ -374,14 +420,13 @@
     step = lax.broadcasted_iota(jnp.int32, (64, 128), 0) % 4
     row16 = lax.broadcasted_iota(jnp.int32, (16, 128), 0)
 
-    def give(stage, b):
-        for i, u in enumerate(STAGES[stage]):
-            away[stage, b, i] = sums[u, 256 + 64 * b : 320 + 64 * b].astype(BF16)
+    def give(u, b):
+        away[u, 64 * b : 64 * b + 64] = sums[u, 256 + 64 * b : 320 + 64 * b].astype(BF16)
 
     def recur(n, b):
         rows = slice(64 * b, 64 * b + 64)
         h = 1 - head if n else head
-        parts = (given[u % 2, b, u // 2] if n else sums[u, rows].astype(BF16) for u in range(4))
+        parts = (given[u, rows] if n else sums[u, rows].astype(BF16) for u in range(4))
         q, p, v, gate = (part.astype(F32) for part in parts)
         q = q * 128 ** -0.5
         g = gate_of(p, bound[:, columns(h)])
@@ -444,8 +489,8 @@
             pltpu.VMEM((16, 512, 256), BF16),
             pltpu.VMEM((4, 16, 256, 128), BF16),
             pltpu.VMEM((4, 512, 128), F32),
-            pltpu.VMEM((2, 4, 2, 64, 128), BF16),
-            pltpu.VMEM((2, 4, 2, 64, 128), BF16),
+            pltpu.VMEM((4, 256, 128), BF16),
+            pltpu.VMEM((4, 256, 128), BF16),
             pltpu.VMEM((64, 2, 128, 128), BF16),
             pltpu.VMEM((64, 128), BF16),
             pltpu.VMEM((64, 128), F32),
@@ -464,7 +509,7 @@
             pltpu.SemaphoreType.DMA((64,)),
             pltpu.SemaphoreType.DMA((16,)),
             pltpu.SemaphoreType.DMA((64,)),
-            pltpu.SemaphoreType.DMA((8,)),
+            pltpu.SemaphoreType.DMA((16,)),
             pltpu.SemaphoreType.DMA((12,)),
             pltpu.SemaphoreType.DMA((8,)),
         ],

time: 60.7 us -> 57.5 us (0.947)
  Pallas kernels: 59.9 us -> 56.6 us
    pallas_call x1, Pallas kernels: 56.4 us -> 53.1 us  [layer_of(): pl.pallas_call(layer_kernel, in_specs=[outside] * 13, out_specs=[pl.Block...]
where the time goes in v4:
time: 57.5 us; the launch traced here: 57.4 us
  Pallas kernels  56.6 us (98%)
  between operations  0.8 us (1%)
    pallas_call x1, Pallas kernels, layer_of(): pl.pallas_call(layer_kernel, in_specs=[outside] * 13, out_specs=[pl.Block...  53.1 us
    pallas_call x1, Pallas kernels, finish_of(): pl.pallas_call(finish_kernel, in_specs=[inside] * 3, out_specs=[anywhere]...  3.49 us

profile of v4, /device:TPU:1, one launch (start us, length us, event | category | flops | bytes accessed | tf_op | source)
XLA Modules:
  0.0 57.4 jit_solution(6355090689206335738)
XLA Ops:
  0.6 53.1 %layer.1 = (f32[64,2,128,128]{3,2,1,0:T(8,128)S(1)}, bf16[16,256,128]{2,1,0:T(8,128)(2,1)S(1)}, bf16[16,128,512]{2,1,0:T(8,128)(2,1)S(1)}) custom-call(s32[64]{0:T(128)} %accepted_in.1, bf16[256,4096]{1,0:T(8,128)(2,1)} %tokens.1, f32[1,4096]{1,0:T(1,128)} %bitcast.3, bf16[256,256]{1,0:T(8,128)(2,1)} %w0.1, bf16[256,256]{1,0:T(8,128)(2,1)} %w1.1, ...), custom_call_target="tpu_custom_call" | custom-call | tf_op jit(solution)/shard_map/layer/pallas_call | solution.py:477
  53.7 3.5 %finish.1 = (bf16[256,512]{1,0:T(8,128)(2,1)}, f32[64,2,128,128]{3,2,1,0:T(8,128)}) custom-call(f32[64,2,128,128]{3,2,1,0:T(8,128)S(1)} %get-tuple-element.5.taken_in, bf16[16,256,128]{2,1,0:T(8,128)(2,1)S(1)} %get-tuple-element.6.heads, bf16[16,128,512]{2,1,0:T(8,128)(2,1)S(1)} %get-tuple-element.7.out_weights), custom_call_target="tpu_custom_call" | custom-call | tf_op jit(solution)/shard_map/finish/pallas_call | solution.py:541

commit v5 on v4

--- a/solution.py
+++ b/solution.py
@@ -14,9 +14,10 @@
 F32, BF16 = jnp.float32, jnp.bfloat16
 
 LAST = 3
+INNER_NOW = (False, True, True, False, True, True, False, False)
 DIRECT = (("h", 1),)
-Z_FIRST, UP = (False, False, True, True, False, False, True, True), (False, True, True, False, True, True, False, False)
-OUT_Z_FIRST, OUT_UP, OUT_BY_INNER = (False, False, True, True), (True, False, True, False), (False, False, True, False)
+Z_FIRST, UP = (False, False, True, True, False, False, True, True), (False, True, True, True, True, False, False, False)
+OUT_Z_FIRST, OUT_UP, OUT_BY_INNER = (True, False, False, True), (False, False, True, False), (True, False, False, False)
 
 
 def shifted(dz, link):
@@ -43,7 +44,7 @@
         way, other = ("z+", "z-") if UP[2 * u + s] else ("z-", "z+")
         along_z = [way, other] if dz == 0 else [way] if dz == (3 if way == "z+" else 1) else []
         if Z_FIRST[2 * u + s]:
-            links = along_z + ["yi"] if dy == 0 else []
+            links = [] if dy else ["yi"] + along_z if INNER_NOW[2 * u + s] else along_z + ["yi"]
         else:
             links = (["yi"] if dy == dz == 0 else []) + along_z
         return [(k, (kind, u, s, shifted(dz, k), 1 if k == "yi" else dy)) for k in links]
@@ -64,9 +65,9 @@
 
 
 SIZE = {"w": 64, "o": 32, "t": 128, "u": 128, "h": 16, "g": 16}
-SLACK = {"w": 0.6, "u": 1.0, "q": 0.5}
-BEGIN_AT, EARLY_AT, OUT_AT = (0, 0, 0, 16), 16, (54, 54)
-FIRST_SENDS = (("w", 1), ("t", 1), ("t", 0), ("w", 2), ("w", 0), ("w", 3))
+SLACK = {"w": 0.3, "u": 1.0, "q": 0.2}
+BEGIN_AT, EARLY_AT, OUT_AT = (0, 0, 0, 8), 24, (50, 56, 54)
+FIRST_SENDS = (("w", 1), ("t", 0), ("t", 1), ("w", 2), ("w", 0), ("w", 3))
 TIMES = {"norm": 0.6, "norm2": 0.15, "take": 0.4, "product": 0.1, "away": 0.05, "recur": 0.4}
 
 
@@ -79,7 +80,10 @@
     products = [([], []) for _ in range(4)]
     left = [[16, 16] for _ in range(4)]
     tokens = 16
-    held, shut = [], {"z+", "z-", "yi"}
+    held, shut = [], {"z", "first z", "yi"}
+
+    def gate(item, link):
+        return ("first z" if OUT_Z_FIRST[item[1]] else "z") if link[0] == "z" else link
     returned, ends = set(), []
 
     def send(item, link, there):
@@ -94,7 +98,7 @@
 
     def go_on(item):
         for link, there in sends(item):
-            if item[0] == "o" and link in shut:
+            if item[0] == "o" and gate(item, link) in shut:
                 held.append((item, link, there))
             else:
                 send(item, link, there)
@@ -111,7 +115,7 @@
 
     def release(*links):
         shut.difference_update(links)
-        for step in [step for step in held if step[1] in links]:
+        for step in [step for step in held if gate(step[0], step[1]) in links]:
             held.remove(step)
             send(*step)
 
@@ -170,7 +174,9 @@
                     for u in range(4):
                         go_on(("o", u, 0, 0))
                 if got == OUT_AT[0]:
-                    release("z+", "z-")
+                    release("z")
+                if got == OUT_AT[2]:
+                    release("first z")
                 if got == OUT_AT[1]:
                     release("yi")
                 if got == 60:

time: 57.5 us -> 57 us (level)
  Pallas kernels: 56.6 us -> 55.9 us
    pallas_call x1, Pallas kernels: 53.1 us -> 52.4 us  [layer_of(): pl.pallas_call(layer_kernel, in_specs=[outside] * 13, out_specs=[pl.Block...]
where the time goes in v5:
time: 57 us; the launch traced here: 56.7 us
  Pallas kernels  55.9 us (98%)
  between operations  0.8 us (1%)
    pallas_call x1, Pallas kernels, layer_of(): pl.pallas_call(layer_kernel, in_specs=[outside] * 13, out_specs=[pl.Block...  52.4 us
    pallas_call x1, Pallas kernels, finish_of(): pl.pallas_call(finish_kernel, in_specs=[inside] * 3, out_specs=[anywhere]...  3.49 us

profile of v5, /device:TPU:1, one launch (start us, length us, event | category | flops | bytes accessed | tf_op | source)
XLA Modules:
  0.0 56.7 jit_solution(1103273669552494192)
XLA Ops:
  0.6 52.4 %layer.1 = (f32[64,2,128,128]{3,2,1,0:T(8,128)S(1)}, bf16[16,256,128]{2,1,0:T(8,128)(2,1)S(1)}, bf16[16,128,512]{2,1,0:T(8,128)(2,1)S(1)}) custom-call(s32[64]{0:T(128)} %accepted_in.1, bf16[256,4096]{1,0:T(8,128)(2,1)} %tokens.1, f32[1,4096]{1,0:T(1,128)} %bitcast.3, bf16[256,256]{1,0:T(8,128)(2,1)} %w0.1, bf16[256,256]{1,0:T(8,128)(2,1)} %w1.1, ...), custom_call_target="tpu_custom_call" | custom-call | tf_op jit(solution)/shard_map/layer/pallas_call | solution.py:483
  53.1 3.5 %finish.1 = (bf16[256,512]{1,0:T(8,128)(2,1)}, f32[64,2,128,128]{3,2,1,0:T(8,128)}) custom-call(f32[64,2,128,128]{3,2,1,0:T(8,128)S(1)} %get-tuple-element.5.taken_in, bf16[16,256,128]{2,1,0:T(8,128)(2,1)S(1)} %get-tuple-element.6.heads, bf16[16,128,512]{2,1,0:T(8,128)(2,1)S(1)} %get-tuple-element.7.out_weights), custom_call_target="tpu_custom_call" | custom-call | tf_op jit(solution)/shard_map/finish/pallas_call | solution.py:547
